TPU v7x, 32 devices: a whole 2x2x4 slice. The times are simulated.
32 devices in a mesh: sp: 16 (over z, y, x), tp: 2 (over core).
Axes of the slice: x: 2, y: 2, z: 4, core: 2. Of those that a mesh axis runs over, the one named last changes fastest.
Arguments:
- mixer_value_rows: bfloat16 [4096, 2048], P('sp', 'tp'), may hold values from -6 to 6
- input_map_rows: bfloat16 [4096, 256], P('sp', 'tp'), may hold values from -6 to 6
- output_map_rows: bfloat16 [4096, 256], P('sp', 'tp'), may hold values from -6 to 6
- gate_preactivation: bfloat16 [4096, 2048], P('sp', 'tp'), may hold values from -25 to 25
- step_preactivation: float32 [4096, 32], P('sp', 'tp'), may hold values from -4 to 4
- position_extra_decay: float32 [4096, 32], P('sp', 'tp'), may hold values from -0.69 to 0
- head_decay_rate: float32 [32], P('tp'), may hold values from 7.8125e-05 to 0.08
- head_direct_term: float32 [32], P('tp'), may hold values from -2.5 to 2.5
- value_taps: bfloat16 [4, 2048], P(None, 'tp'), may hold values from -3 to 3
- input_map_taps: bfloat16 [4, 256], P(None, 'tp'), may hold values from -3 to 3
- output_map_taps: bfloat16 [4, 256], P(None, 'tp'), may hold values from -3 to 3
- document_index: int32 [4096], P('sp'), may hold values from 0 to 3, never falling along the last dimension, each value on 1 to 1536 neighbouring positions
- gated_norm_gain: float32 [2048], replicated, may hold values from 0.1 to 1.9
- residual: bfloat16 [4096, 2048], P(('sp', 'tp')), may hold values from -6 to 6
- mixer_output_weight: bfloat16 [2048, 2048], replicated, may hold values from -0.125 to 0.125
- expert_norm_gain: float32 [2048], replicated, may hold values from 0.1 to 1.9
- expert_group_weight: float32 [4096, 4], P(('sp', 'tp')), may hold values from 0.5 to 2
- chosen_expert_weight: float32 [4096, 2], P(('sp', 'tp')), may hold values from 0.5 to 2
- chosen_expert_index: int32 [4096, 2], P(('sp', 'tp')), may hold values from 0 to 31, all different within a row; in each aligned block of 128 rows (0 to 127, 128 to 255, ...) at most 16 rows name the same one
- expert_gate_weight: bfloat16 [32, 2048, 512], P(('sp', 'tp')), may hold values from -0.125 to 0.125
- expert_up_weight: bfloat16 [32, 2048, 512], P(('sp', 'tp')), may hold values from -0.125 to 0.125
- expert_down_weight: bfloat16 [32, 512, 2048], P(('sp', 'tp')), may hold values from -0.25 to 0.25
Outputs:
- output: bfloat16 [4096, 2048], P(('sp', 'tp'))
Inputs may be any that keep to these rules, and one draw needn't show every extreme that they name: `document_index`: document numbers never fall along the sequence; a document holds 1 to 1536 positions. `chosen_expert_index`: the 2 entries of a row differ. Among the rows of one device (aligned blocks of 128 rows) no expert is named by more than 16 rows, a bound that some expert reaches in some blocks.
All inputs are finite; a program needn't handle non-finite values.
Results may differ from a plain program's by a relative error of at most 0.019.
Values may be sent and summed in bfloat16 or wider, within the bound.
A program may use at most 128 MiB of HBM per device.

v0:
```python
import functools

import jax
import jax.numpy as jnp
import numpy as np
from jax import lax
from jax.experimental import pallas as pl
from jax.experimental.pallas import tpu as pltpu
from jax.sharding import PartitionSpec as P

D_STATE = 128
EXPERT_GROUPS = 4
LONGEST = 1536
EPSILON = 1e-06

NEG = -1e30
MESH_ID = pl.DeviceIdType.MESH
OFFSETS = (1, 2, 5)


def softplus(v):
    return jnp.maximum(v, 0.0) + jnp.log1p(jnp.exp(-jnp.abs(v)))


def silu(v):
    return v / (1.0 + jnp.exp(-v))


def exact_dot(a, b):
    return jnp.dot(a, b, preferred_element_type=jnp.float32, precision=lax.Precision.HIGHEST)


def mixer_kernel(
    n, x_hbm, b_hbm, c_hbm, gate_hbm, step_hbm, extra_hbm, docs_hbm, resid_hbm, w_hbm,
    rate_ref, direct_ref, spread_ref, taps_ref, btaps_ref, ctaps_ref, docrow_ref, gain_ref,
    gain2_ref,
    mixed_ref, ffn_ref,
    x_ref, b_ref, c_ref, gate_ref, step_ref, extra_ref, docs_ref, resid_ref, w_ref, pad, pad_docs, edge_x, edge_b, edge_c, edge_d,
    vconv, bconv, cconv, ylocal, cumx, s32, t0, t1, t2, g0, g1, g2,
    r0, r1, r1far, r2, rg0, rg1, rg2, gated, regrouped,
    wsem, send, recv,
):
    sp = lax.axis_index("sp")
    tp = lax.axis_index("tp")
    length, channels = x_ref.shape
    state = b_ref.shape[1]
    lanes = 128
    chunks = channels // lanes
    heads = step_ref.shape[1]
    half = length // 2
    edge = edge_x.shape[0]

    loads = [
        pltpu.make_async_copy(source, target, wsem.at[i])
        for i, (source, target) in enumerate((
            (x_hbm, x_ref), (b_hbm, b_ref), (c_hbm, c_ref), (docs_hbm, docs_ref),
            (step_hbm, step_ref), (extra_hbm, extra_ref), (gate_hbm, gate_ref),
            (resid_hbm, resid_ref), (w_hbm, w_ref),
        ))
    ]
    for load in loads:
        load.start()

    barrier = pltpu.get_barrier_semaphore()
    count = jnp.int32(1)
    pl.semaphore_signal(barrier, inc=1, device_id=(sp, 1 - tp), device_id_type=MESH_ID)
    for off in OFFSETS:
        @pl.when(sp + off < n)
        def _():
            pl.semaphore_signal(barrier, inc=1, device_id=(sp + off, tp), device_id_type=MESH_ID)

        @pl.when(sp >= off)
        def _():
            pl.semaphore_signal(barrier, inc=1, device_id=(sp - off, tp), device_id_type=MESH_ID)

        count = count + (sp + off < n).astype(jnp.int32) + (sp >= off).astype(jnp.int32)
    pl.semaphore_wait(barrier, count)

    def copy(slot, src, dst, off):
        return pltpu.make_async_remote_copy(
            src_ref=src, dst_ref=dst, send_sem=send.at[slot], recv_sem=recv.at[slot],
            device_id=(sp + off, tp), device_id_type=MESH_ID,
        )

    last = pl.ds(length - edge, edge)
    edges = [
        copy(0, x_ref.at[last, :], edge_x, 1),
        copy(1, b_ref.at[last, :], edge_b, 1),
        copy(2, c_ref.at[last, :], edge_c, 1),
        copy(3, docs_ref.at[last, :], edge_d, 1),
    ]

    def start(copies, off):
        @pl.when(sp + off < n)
        def _():
            for one in copies:
                one.start()

    def wait_recv(copies, off):
        @pl.when(sp >= off)
        def _():
            for one in copies:
                one.wait_recv()

    def wait_send(copies, off):
        @pl.when(sp + off < n)
        def _():
            for one in copies:
                one.wait_send()

    for load in loads[:4]:
        load.wait()
    start(edges, 1)
    for load in loads[4:6]:
        load.wait()

    step = softplus(step_ref[...])
    logs = extra_ref[...] - step * rate_ref[...]
    rows = lax.broadcasted_iota(jnp.int32, (length, length), 0)
    cols = lax.broadcasted_iota(jnp.int32, (length, length), 1)
    causal = rows >= cols
    cum = exact_dot(causal.astype(jnp.float32), logs)
    cum_t = lax.dot_general(
        logs, (rows <= cols).astype(jnp.float32), (((0,), (0,)), ((), ())),
        preferred_element_type=jnp.float32, precision=lax.Precision.HIGHEST,
    )
    same = docs_ref[:, 0:1] == docrow_ref[0:1, :]
    blocked = jnp.where(causal & same, 0.0, NEG)
    tail = (docs_ref[...] == docs_ref[length - 1 : length, :]).astype(jnp.float32)

    pad[edge:, :channels] = x_ref[...].astype(jnp.float32)
    pad[edge:, channels : channels + state] = b_ref[...].astype(jnp.float32)
    pad[edge:, channels + state :] = c_ref[...].astype(jnp.float32)
    pad_docs[edge:, :] = docs_ref[...]

    wait_recv(edges, 1)
    has = sp >= 1
    pad[:edge, :channels] = jnp.where(has, edge_x[...].astype(jnp.float32), 0.0)
    pad[:edge, channels : channels + state] = jnp.where(has, edge_b[...].astype(jnp.float32), 0.0)
    pad[:edge, channels + state :] = jnp.where(has, edge_c[...].astype(jnp.float32), 0.0)
    pad_docs[:edge, :] = jnp.where(has, edge_d[...], 0.0)

    taps_count = taps_ref.shape[0]
    base = edge - taps_count + 1
    masks = [
        (pad_docs[base + k : base + k + length, :] == docs_ref[...]).astype(jnp.float32)
        for k in range(taps_count - 1)
    ]

    def conv(at, taps, start_lane):
        total = taps[taps_count - 1 :, start_lane : start_lane + lanes].astype(
            jnp.float32
        ) * pad[edge : edge + length, at : at + lanes]
        for k in range(taps_count - 1):
            total = total + (
                taps[k : k + 1, start_lane : start_lane + lanes].astype(jnp.float32)
                * pad[base + k : base + k + length, at : at + lanes]
                * masks[k]
            )
        return silu(total).astype(jnp.bfloat16)

    bconv[...] = conv(channels, btaps_ref, 0)
    cconv[...] = conv(channels + state, ctaps_ref, 0)

    keep = (docs_ref[length - 1 : length, :] == pad_docs[edge - 1 : edge, :]).astype(jnp.float32)
    keep = keep * has.astype(jnp.float32)
    b_t = jnp.transpose(bconv[...].astype(jnp.float32)).astype(jnp.bfloat16)
    for j in range(chunks):
        at = slice(j * lanes, (j + 1) * lanes)
        value = conv(j * lanes, taps_ref, j * lanes)
        vconv[:, at] = value
        widen = spread_ref[:, at]
        cum_wide = exact_dot(cum, widen)
        cumx[:, at] = cum_wide
        stepped = (exact_dot(step, widen) * value.astype(jnp.float32)).astype(jnp.bfloat16)
        ylocal[:, at] = stepped.astype(jnp.float32)
        ending = cum_wide[length - 1 : length, :]
        ended = (jnp.exp(ending - cum_wide) * tail * stepped.astype(jnp.float32)).astype(
            jnp.bfloat16
        )
        fresh = jnp.dot(b_t, ended, preferred_element_type=jnp.float32)
        s32[:, at] = fresh
        t0[:, at] = fresh.astype(jnp.bfloat16)
        g0[:, at] = jnp.broadcast_to(jnp.exp(ending) * keep, (8, lanes))
    first = [copy(4, t0, r0, 1), copy(5, g0, rg0, 1)]
    start(first, 1)

    scores = lax.dot_general(
        cconv[...], bconv[...], (((1,), (1,)), ((), ())), preferred_element_type=jnp.float32
    )
    per_chunk = heads // chunks
    width = lanes // per_chunk
    lane = lax.broadcasted_iota(jnp.int32, (length, lanes), 1)

    def inside(j):
        at = slice(j * lanes, (j + 1) * lanes)
        stepped = ylocal[:, at].astype(jnp.bfloat16)
        result = None
        for k in range(per_chunk):
            h = j * per_chunk + k
            decay = jnp.exp(cum[:, h : h + 1] - cum_t[h : h + 1, :] + blocked)
            part = jnp.dot(
                (scores * decay).astype(jnp.bfloat16), stepped, preferred_element_type=jnp.float32
            )
            result = part if result is None else jnp.where(lane < k * width, result, part)
        direct = direct_ref[:, at]
        ylocal[:, at] = result + direct * vconv[:, at].astype(jnp.float32)

    third = chunks // 3
    for j in range(third):
        inside(j)

    wait_recv(first, 1)
    grow0 = g0[0:1, :]
    before = jnp.where(has, r0[...].astype(jnp.float32), 0.0)
    s32[...] = s32[...] + grow0 * before
    t1[...] = s32[...].astype(jnp.bfloat16)
    g1[...] = g0[...] * jnp.where(has, rg0[...], 0.0)
    second = [copy(6, t1, r1, 2), copy(7, g1, rg1, 2)]
    far = [copy(8, t1, r1far, 5)]
    start(second, 2)
    start(far, 5)
    for j in range(third, 2 * third):
        inside(j)

    wait_recv(second, 2)
    has2 = sp >= 2
    before = jnp.where(has2, r1[...].astype(jnp.float32), 0.0)
    t2[...] = (s32[...] + g1[0:1, :] * before).astype(jnp.bfloat16)
    g2[...] = g1[...] * jnp.where(has2, rg1[...], 0.0)
    final = [copy(9, t2, r2, 1), copy(10, g2, rg2, 1)]
    start(final, 1)
    for j in range(2 * third, chunks):
        inside(j)

    wait_recv(final, 1)
    wait_recv(far, 5)
    has5 = sp >= 5
    incoming = (
        jnp.where(has, r2[...].astype(jnp.float32), 0.0)
        + jnp.where(has, rg2[0:1, :], 0.0) * jnp.where(has5, r1far[...].astype(jnp.float32), 0.0)
    ).astype(jnp.bfloat16)
    loads[6].wait()
    entering = (docs_ref[...] == pad_docs[edge - 1 : edge, :]).astype(jnp.float32)
    for j in range(chunks):
        at = slice(j * lanes, (j + 1) * lanes)
        readout = jnp.dot(cconv[...], incoming[:, at], preferred_element_type=jnp.float32)
        whole = ylocal[:, at] + readout * jnp.exp(cumx[:, at]) * entering
        gated[:, at] = (whole * silu(gate_ref[:, at].astype(jnp.float32))).astype(jnp.bfloat16)

    swap = pltpu.make_async_remote_copy(
        src_ref=gated.at[pl.ds(pl.multiple_of((1 - tp) * half, half), half), :],
        dst_ref=regrouped,
        send_sem=send.at[11], recv_sem=recv.at[11],
        device_id=(sp, 1 - tp), device_id_type=MESH_ID,
    )
    swap.start()
    wait_send(edges, 1)
    wait_send(first, 1)
    wait_send(second, 2)
    wait_send(far, 5)
    wait_send(final, 1)
    loads[7].wait()
    loads[8].wait()
    swap.wait()
    own = gated[pl.ds(pl.multiple_of(tp * half, half), half), :].astype(jnp.float32)
    other = regrouped[...].astype(jnp.float32)
    total = jnp.sum(own * own, axis=-1, keepdims=True) + jnp.sum(other * other, axis=-1, keepdims=True)
    features = 2 * channels
    factor = lax.rsqrt(total / features + EPSILON)
    low = jnp.where(tp == 0, own, other)
    high = jnp.where(tp == 0, other, own)
    low = (low * factor * gain_ref[:, :channels]).astype(jnp.bfloat16)
    high = (high * factor * gain_ref[:, channels:]).astype(jnp.bfloat16)
    square = jnp.zeros((half, 1), jnp.float32)
    piece = 512
    model = resid_ref.shape[1]
    for j in range(model // piece):
        at = slice(j * piece, (j + 1) * piece)
        projected = jnp.dot(low, w_ref[:channels, at], preferred_element_type=jnp.float32)
        projected += jnp.dot(high, w_ref[channels:, at], preferred_element_type=jnp.float32)
        mixed = (resid_ref[:, at].astype(jnp.float32) + projected).astype(jnp.bfloat16)
        mixed_ref[:, at] = mixed
        wide = mixed.astype(jnp.float32)
        square += jnp.sum(wide * wide, axis=-1, keepdims=True)
    factor = lax.rsqrt(square / model + EPSILON)
    ffn_ref[...] = (mixed_ref[...].astype(jnp.float32) * factor * gain2_ref[...]).astype(jnp.bfloat16)


def mixer(n, x, b, c, gate, step, extra, rate, direct, taps, btaps, ctaps, docs, gain, resid,
          weight, gain2):
    length, channels = x.shape
    state = b.shape[1]
    heads = step.shape[1]
    width = channels // heads
    model = resid.shape[1]
    half = resid.shape[0]
    assert state == D_STATE and (LONGEST - 2) // length + 1 <= 6
    marks = (docs + 1).astype(jnp.float32)
    docs_wide = jnp.broadcast_to(marks[:, None], (length, 128))
    docs_row = jnp.broadcast_to(marks[None, :], (8, length))
    spread = jnp.asarray(np.repeat(np.eye(heads, dtype=np.float32), width, axis=1))
    direct_wide = jnp.repeat(direct, width)[None, :]
    bf, f32 = jnp.bfloat16, jnp.float32
    edge = 16
    vm = pltpu.VMEM
    return pl.pallas_call(
        functools.partial(mixer_kernel, n),
        out_shape=[jax.ShapeDtypeStruct((half, model), bf)] * 2,
        in_specs=[pl.BlockSpec(memory_space=pl.ANY)] * 9
        + [pl.BlockSpec(memory_space=pltpu.VMEM)] * 9,
        out_specs=[pl.BlockSpec(memory_space=pltpu.VMEM)] * 2,
        scratch_shapes=[
            vm(x.shape, bf), vm(b.shape, bf), vm(c.shape, bf), vm(gate.shape, bf),
            vm(step.shape, f32), vm(extra.shape, f32), vm(docs_wide.shape, f32),
            vm(resid.shape, bf), vm(weight.shape, bf),
            vm((edge + length, channels + 2 * state), f32), vm((edge + length, 128), f32),
            vm((edge, channels), bf), vm((edge, state), bf), vm((edge, state), bf),
            vm((edge, 128), f32),
            vm((length, channels), bf), vm((length, state), bf), vm((length, state), bf),
            vm((length, channels), f32), vm((length, channels), f32),
            vm((state, channels), f32),
            vm((state, channels), bf), vm((state, channels), bf), vm((state, channels), bf),
            vm((8, channels), f32), vm((8, channels), f32), vm((8, channels), f32),
            vm((state, channels), bf), vm((state, channels), bf), vm((state, channels), bf),
            vm((state, channels), bf),
            vm((8, channels), f32), vm((8, channels), f32), vm((8, channels), f32),
            vm((length, channels), bf), vm((half, channels), bf),
            pltpu.SemaphoreType.DMA((9,)), pltpu.SemaphoreType.DMA((12,)), pltpu.SemaphoreType.DMA((12,)),
        ],
        compiler_params=pltpu.CompilerParams(
            collective_id=0, has_side_effects=True, vmem_limit_bytes=58 * 1024 * 1024
        ),
    )(x, b, c, gate, step, extra, docs_wide, resid, weight, rate[None, :], direct_wide, spread,
      taps, btaps, ctaps, docs_row, gain[None, :], gain2[None, :])


def expert_kernel(
    n, tps, ffn_ref, pick_ref, high_ref, low_ref, mixed_ref, wg_hbm, wu_hbm, wd_hbm, out_ref,
    wg, wu, wd, slots, arrived, done, back, wsem, local, fsend, frecv, bsend, brecv,
):
    sp = lax.axis_index("sp")
    tp = lax.axis_index("tp")
    me = sp * tps + tp
    cap = slots.shape[0] // n
    loads = [
        pltpu.make_async_copy(wg_hbm.at[0], wg, wsem.at[0]),
        pltpu.make_async_copy(wu_hbm.at[0], wu, wsem.at[1]),
        pltpu.make_async_copy(wd_hbm.at[0], wd, wsem.at[2]),
    ]
    for load in loads:
        load.start()

    def place(device):
        return (device // tps, device % tps)

    barrier = pltpu.get_barrier_semaphore()

    def greet(k, carry):
        pl.semaphore_signal(
            barrier, inc=1, device_id=place((me + k) % n), device_id_type=MESH_ID
        )
        return carry

    lax.fori_loop(1, n, greet, 0)
    piece = 512
    model = ffn_ref.shape[1]
    for j in range(model // piece):
        at = slice(j * piece, (j + 1) * piece)
        slots[:, at] = jnp.dot(
            pick_ref[...], ffn_ref[:, at], preferred_element_type=jnp.float32
        ).astype(jnp.bfloat16)
    pl.semaphore_wait(barrier, n - 1)

    def rows(index):
        return pl.ds(pl.multiple_of(index * cap, cap), cap)

    def forward(k):
        target = (me + k) % n
        return pltpu.make_async_remote_copy(
            src_ref=slots.at[rows(target), :], dst_ref=arrived.at[rows(k), :],
            send_sem=fsend.at[k], recv_sem=frecv.at[k],
            device_id=place(target), device_id_type=MESH_ID,
        )

    def backward(k):
        return pltpu.make_async_remote_copy(
            src_ref=done.at[rows(k), :], dst_ref=back.at[rows(me), :],
            send_sem=bsend.at[k], recv_sem=brecv.at[k],
            device_id=place((me + n - k) % n), device_id_type=MESH_ID,
        )

    def returned(k):
        return pltpu.make_async_remote_copy(
            src_ref=done.at[rows(k), :], dst_ref=back.at[rows((me + k) % n), :],
            send_sem=bsend.at[k], recv_sem=brecv.at[k],
            device_id=place((me + n - k) % n), device_id_type=MESH_ID,
        )

    def loop(low, high, act):
        def body(k, carry):
            act(k)
            return carry

        lax.fori_loop(low, high, body, 0)

    loop(1, n, lambda k: forward(k).start())
    own = pltpu.make_async_copy(slots.at[rows(me), :], arrived.at[rows(0), :], local.at[0])
    own.start()
    own.wait()
    for load in loads:
        load.wait()
    groups = 8 if n % 8 == 0 else 4
    size = n // groups
    for g in range(groups):
        low = g * size
        loop(max(low, 1), low + size, lambda k: forward(k).wait_recv())
        part = slice(low * cap, (low + size) * cap)
        tokens = arrived[part, :]
        gate = jnp.dot(tokens, wg[...], preferred_element_type=jnp.float32)
        up = jnp.dot(tokens, wu[...], preferred_element_type=jnp.float32)
        hidden = (silu(gate) * up).astype(jnp.bfloat16)
        for j in range(model // piece):
            at = slice(j * piece, (j + 1) * piece)
            done[part, at] = jnp.dot(
                hidden, wd[:, at], preferred_element_type=jnp.float32
            ).astype(jnp.bfloat16)
        loop(max(low, 1), low + size, lambda k: backward(k).start())
    mine = pltpu.make_async_copy(done.at[rows(0), :], back.at[rows(me), :], local.at[1])
    mine.start()
    mine.wait()
    loop(1, n, lambda k: forward(k).wait_send())
    loop(1, n, lambda k: returned(k).wait_recv())
    for j in range(model // piece):
        at = slice(j * piece, (j + 1) * piece)
        total = mixed_ref[:, at].astype(jnp.float32)
        total += jnp.dot(high_ref[...], back[:, at], preferred_element_type=jnp.float32)
        total += jnp.dot(low_ref[...], back[:, at], preferred_element_type=jnp.float32)
        out_ref[:, at] = total.astype(jnp.bfloat16)
    loop(1, n, lambda k: backward(k).wait_send())


def exchange(ffn, pick, high, low, mixed, gate_weight, up_weight, down_weight):
    n = lax.axis_size("sp") * lax.axis_size("tp")
    slots, model = pick.shape[0], ffn.shape[1]
    bf = jnp.bfloat16
    vm = pltpu.VMEM
    return pl.pallas_call(
        functools.partial(expert_kernel, n, lax.axis_size("tp")),
        out_shape=jax.ShapeDtypeStruct(mixed.shape, bf),
        in_specs=[pl.BlockSpec(memory_space=pltpu.VMEM)] * 5
        + [pl.BlockSpec(memory_space=pl.ANY)] * 3,
        out_specs=pl.BlockSpec(memory_space=pltpu.VMEM),
        scratch_shapes=[
            vm(gate_weight.shape[1:], bf), vm(up_weight.shape[1:], bf),
            vm(down_weight.shape[1:], bf),
            vm((slots, model), bf), vm((slots, model), bf), vm((slots, model), bf),
            vm((slots, model), bf),
            pltpu.SemaphoreType.DMA((3,)), pltpu.SemaphoreType.DMA((2,)),
            pltpu.SemaphoreType.DMA((n,)), pltpu.SemaphoreType.DMA((n,)),
            pltpu.SemaphoreType.DMA((n,)), pltpu.SemaphoreType.DMA((n,)),
        ],
        compiler_params=pltpu.CompilerParams(
            collective_id=1, has_side_effects=True, vmem_limit_bytes=56 * 1024 * 1024
        ),
    )(ffn, pick, high, low, mixed, gate_weight, up_weight, down_weight)


def local(
    mixer_value_rows,
    input_map_rows,
    output_map_rows,
    gate_preactivation,
    step_preactivation,
    position_extra_decay,
    head_decay_rate,
    head_direct_term,
    value_taps,
    input_map_taps,
    output_map_taps,
    document_index,
    gated_norm_gain,
    residual,
    mixer_output_weight,
    expert_norm_gain,
    expert_group_weight,
    chosen_expert_weight,
    chosen_expert_index,
    expert_gate_weight,
    expert_up_weight,
    expert_down_weight,
):
    mixed_rows, ffn_in = mixer(
        lax.axis_size("sp"), mixer_value_rows, input_map_rows, output_map_rows,
        gate_preactivation, step_preactivation, position_extra_decay, head_decay_rate,
        head_direct_term, value_taps, input_map_taps, output_map_taps, document_index,
        gated_norm_gain, residual, mixer_output_weight, expert_norm_gain,
    )
    experts = lax.axis_size("sp") * lax.axis_size("tp")
    row_count, width = ffn_in.shape
    choose = chosen_expert_index.shape[1]
    capacity = 2 * mixer_value_rows.shape[0] // experts
    ids = jnp.arange(experts, dtype=jnp.int32)
    chosen = (chosen_expert_index[:, :, None] == ids).astype(jnp.bfloat16)
    named = jnp.sum(chosen, axis=1)
    below = jnp.asarray(np.tril(np.ones((row_count, row_count), np.float32), -1), jnp.bfloat16)
    rank = jnp.dot(below, named, preferred_element_type=jnp.float32).astype(jnp.int32)
    per_expert_group = experts // EXPERT_GROUPS
    group_of = jnp.asarray(np.repeat(np.eye(EXPERT_GROUPS, dtype=np.float32), per_expert_group, axis=1))
    group_weight = jnp.sum(expert_group_weight[:, :, None] * group_of[None], axis=1)
    weight = group_weight * jnp.sum(
        chosen.astype(jnp.float32) * chosen_expert_weight[:, :, None], axis=1
    )
    hot = (rank[:, :, None] == jnp.arange(capacity, dtype=jnp.int32)) & (named[:, :, None] > 0)
    pick = hot.astype(jnp.bfloat16).reshape(row_count, experts * capacity)
    route = jnp.where(hot, weight[:, :, None], 0.0).reshape(row_count, experts * capacity)
    route_high = route.astype(jnp.bfloat16)
    route_low = (route - route_high.astype(jnp.float32)).astype(jnp.bfloat16)
    if capacity % 16 == 0 and experts % 4 == 0:
        return exchange(
            ffn_in, pick.T, route_high, route_low, mixed_rows,
            expert_gate_weight, expert_up_weight, expert_down_weight,
        )
    outgoing = lax.dot_general(
        pick, ffn_in, (((0,), (0,)), ((), ())), preferred_element_type=jnp.float32
    ).astype(jnp.bfloat16)
    received = lax.all_to_all(
        outgoing.reshape(experts, capacity, width), ("sp", "tp"), split_axis=0, concat_axis=0,
        tiled=True,
    )
    flat_rows = received.reshape(-1, width)
    gate_part = jnp.dot(flat_rows, expert_gate_weight[0], preferred_element_type=jnp.float32)
    upward = jnp.dot(flat_rows, expert_up_weight[0], preferred_element_type=jnp.float32)
    hidden = (jax.nn.silu(gate_part) * upward).astype(jnp.bfloat16)
    finished = jnp.dot(
        hidden, expert_down_weight[0], preferred_element_type=jnp.float32
    ).astype(jnp.bfloat16)
    returned = lax.all_to_all(
        finished.reshape(received.shape), ("sp", "tp"), split_axis=0, concat_axis=0, tiled=True
    ).reshape(experts * capacity, width)
    summed = (
        mixed_rows.astype(jnp.float32)
        + jnp.dot(route_high, returned, preferred_element_type=jnp.float32)
        + jnp.dot(route_low, returned, preferred_element_type=jnp.float32)
    )
    return summed.astype(jnp.bfloat16)


def solution(mesh):
    placed = (
        P("sp", "tp"),
        P("sp", "tp"),
        P("sp", "tp"),
        P("sp", "tp"),
        P("sp", "tp"),
        P("sp", "tp"),
        P("tp"),
        P("tp"),
        P(None, "tp"),
        P(None, "tp"),
        P(None, "tp"),
        P("sp"),
        P(),
        P(("sp", "tp"), None),
        P(),
        P(),
        P(("sp", "tp"), None),
        P(("sp", "tp"), None),
        P(("sp", "tp"), None),
        P(("sp", "tp"), None, None),
        P(("sp", "tp"), None, None),
        P(("sp", "tp"), None, None),
    )
    return jax.shard_map(
        local, mesh=mesh, in_specs=placed, out_specs=P(("sp", "tp"), None), check_vma=False
    )
```

profile of v0, /device:TPU:0, one launch (start us, length us, event | category | flops | bytes accessed | tf_op | source)
XLA Modules:
  0.0 173.4 jit_solution(16776213535725169530)
XLA Ops:
  0.0 0.7 add_convert_fusion
  0.7 0.7 fusion.2
  1.4 0.9 fusion
  2.3 0.6 broadcast_in_dim.50.docrow_ref
  2.9 0.7 broadcast_in_dim.24
  3.6 0.7 broadcast_in_dim_reshape.3.direct_ref
  4.3 0.8 multiply_reduce_fusion
  5.1 0.7 multiply_reduce_fusion.1
  5.8 0.1 eq.40
  5.9 0.2 copy.45
  6.1 0.8 broadcast_in_dim.22.docs_hbm
  6.8 1.5 copy.42.step_hbm
  8.3 1.5 copy.43.extra_hbm
  9.8 0.1 copy.46
  9.9 0.1 copy.44
  10.1 0.7 subtract_convert_fusion
  10.8 0.7 select_convert_fusion.high_ref
  11.5 0.8 copy.47.pick_ref
  12.3 31.7 %shard_map.235 = (bf16[128,2048]{1,0:T(8,128)(2,1)}, bf16[128,2048]{1,0:T(8,128)(2,1)}) custom-call(bf16[256,1024]{1,0:T(8,128)(2,1)} %x_hbm.1, bf16[256,128]{1,0:T(8,128)(2,1)} %b_hbm.1, bf16[256,128]{1,0:T(8,128)(2,1)} %c_hbm.1, bf16[256,1024]{1,0:T(8,128)(2,1)} %gate_hbm.1, f32[256,16]{1,0:T(8,128)} %copy.42.step_hbm, f32[256,16]{1,0:T(8,128)} %copy.43.extra_hbm, ...), custom_call_target="tpu_custom_call" | custom-call | tf_op jit(solution)/shard_map/pallas_call | solution.py:307
  43.9 127.6 %shard_map.236 = bf16[128,2048]{1,0:T(8,128)(2,1)} custom-call(bf16[128,2048]{1,0:T(8,128)(2,1)} %get-tuple-element.7.ffn_ref, bf16[512,128]{1,0:T(8,128)(2,1)} %copy.47.pick_ref, bf16[128,512]{1,0:T(8,128)(2,1)} %select_convert_fusion.high_ref, bf16[128,512]{1,0:T(8,128)(2,1)} %get-tuple-element.9.low_ref, bf16[128,2048]{1,0:T(8,128)(2,1)} %get-tuple-element.8.mixed_ref, ...), custom_call_target="tpu_custom_call" | custom-call | tf_op jit(solution)/shard_map/pallas_call | solution.py:448
  171.5 1.9 %copy.49 = bf16[128,2048]{1,0:T(8,128)(2,1)} copy(bf16[128,2048]{1,0:T(8,128)(2,1)} %shard_map.236) | data formatting | bytes 1048576
  (7 shorter events, 0.1 us)
where the time goes:
time: 174 us; the launch traced here: 173 us
  Pallas kernels  159 us (91%)
  local copies, waits for them, and re-layouts  8.9 us (5%)
  other arithmetic  4.29 us (2%)
    pallas_call x1, Pallas kernels, exchange(): pl.pallas_call(functools.partial(expert_kernel, n, lax.axis_size('tp')),...  128 us
    pallas_call x1, Pallas kernels, mixer(): pl.pallas_call(functools.partial(mixer_kernel, n), out_shape=[jax.ShapeDt...  31.7 us
    unnamed x3, local copies, waits for them, and re-layouts  4.81 us

commit v1 on v0

--- a/solution.py
+++ b/solution.py
@@ -335,14 +335,24 @@
       taps, btaps, ctaps, docs_row, gain[None, :], gain2[None, :])
 
 
-def expert_kernel(
-    n, tps, ffn_ref, pick_ref, high_ref, low_ref, mixed_ref, wg_hbm, wu_hbm, wd_hbm, out_ref,
-    wg, wu, wd, slots, arrived, done, back, wsem, local, fsend, frecv, bsend, brecv,
+def plane_kernel(
+    planes, tps, ffn_ref, ids_ref, group_ref, weight_ref, mixed_ref, wg_hbm, wu_hbm, wd_hbm,
+    out_ref,
+    wg, wu, wd, meta, picks, routes, line, slots, arrived, done, back, part, mine, parts,
+    wsem, msend, mrecv, lsend, lrecv, fsend, frecv, bsend, brecv, psend, precv,
 ):
     sp = lax.axis_index("sp")
     tp = lax.axis_index("tp")
-    me = sp * tps + tp
-    cap = slots.shape[0] // n
+    rows, model = ffn_ref.shape
+    per = lax.axis_size("sp") * tps // planes
+    hosts = per // tps
+    cap = rows // per
+    experts = planes * per
+    chunks = lrecv.shape[1]
+    width = model // chunks
+    z = sp // hosts
+    q = (sp % hosts) * tps + tp
+
     loads = [
         pltpu.make_async_copy(wg_hbm.at[0], wg, wsem.at[0]),
         pltpu.make_async_copy(wu_hbm.at[0], wu, wsem.at[1]),
@@ -351,51 +361,8 @@
     for load in loads:
         load.start()
 
-    def place(device):
-        return (device // tps, device % tps)
-
-    barrier = pltpu.get_barrier_semaphore()
-
-    def greet(k, carry):
-        pl.semaphore_signal(
-            barrier, inc=1, device_id=place((me + k) % n), device_id_type=MESH_ID
-        )
-        return carry
-
-    lax.fori_loop(1, n, greet, 0)
-    piece = 512
-    model = ffn_ref.shape[1]
-    for j in range(model // piece):
-        at = slice(j * piece, (j + 1) * piece)
-        slots[:, at] = jnp.dot(
-            pick_ref[...], ffn_ref[:, at], preferred_element_type=jnp.float32
-        ).astype(jnp.bfloat16)
-    pl.semaphore_wait(barrier, n - 1)
-
-    def rows(index):
-        return pl.ds(pl.multiple_of(index * cap, cap), cap)
-
-    def forward(k):
-        target = (me + k) % n
-        return pltpu.make_async_remote_copy(
-            src_ref=slots.at[rows(target), :], dst_ref=arrived.at[rows(k), :],
-            send_sem=fsend.at[k], recv_sem=frecv.at[k],
-            device_id=place(target), device_id_type=MESH_ID,
-        )
-
-    def backward(k):
-        return pltpu.make_async_remote_copy(
-            src_ref=done.at[rows(k), :], dst_ref=back.at[rows(me), :],
-            send_sem=bsend.at[k], recv_sem=brecv.at[k],
-            device_id=place((me + n - k) % n), device_id_type=MESH_ID,
-        )
-
-    def returned(k):
-        return pltpu.make_async_remote_copy(
-            src_ref=done.at[rows(k), :], dst_ref=back.at[rows((me + k) % n), :],
-            send_sem=bsend.at[k], recv_sem=brecv.at[k],
-            device_id=place((me + n - k) % n), device_id_type=MESH_ID,
-        )
+    def place(plane, member):
+        return (plane * hosts + member // tps, member % tps)
 
     def loop(low, high, act):
         def body(k, carry):
@@ -404,49 +371,260 @@
 
         lax.fori_loop(low, high, body, 0)
 
-    loop(1, n, lambda k: forward(k).start())
-    own = pltpu.make_async_copy(slots.at[rows(me), :], arrived.at[rows(0), :], local.at[0])
-    own.start()
-    own.wait()
-    for load in loads:
-        load.wait()
-    groups = 8 if n % 8 == 0 else 4
-    size = n // groups
-    for g in range(groups):
-        low = g * size
-        loop(max(low, 1), low + size, lambda k: forward(k).wait_recv())
-        part = slice(low * cap, (low + size) * cap)
-        tokens = arrived[part, :]
+    barrier = pltpu.get_barrier_semaphore()
+
+    def greet(device):
+        pl.semaphore_signal(barrier, inc=1, device_id=device, device_id_type=MESH_ID)
+
+    loop(1, per, lambda d: greet(place(z, (q + d) % per)))
+    loop(1, planes, lambda d: greet(place((z + d) % planes, q)))
+
+    def columns(c):
+        return pl.ds(pl.multiple_of(c * width, width), width)
+
+    def member_rows(member):
+        return pl.ds(pl.multiple_of(member * cap, cap), cap)
+
+    def tell(plane, target):
+        return pltpu.make_async_remote_copy(
+            src_ref=meta.at[plane], dst_ref=meta.at[plane],
+            send_sem=msend.at[target], recv_sem=mrecv.at[plane],
+            device_id=place(target, q), device_id_type=MESH_ID,
+        )
+
+    def hop(plane, c, up):
+        return pltpu.make_async_remote_copy(
+            src_ref=line.at[plane, :, columns(c)], dst_ref=line.at[plane, :, columns(c)],
+            send_sem=lsend.at[up, plane, c], recv_sem=lrecv.at[plane, c],
+            device_id=place(z + 2 * up - 1, q), device_id_type=MESH_ID,
+        )
+
+    def forward(plane, c, member):
+        return pltpu.make_async_remote_copy(
+            src_ref=slots.at[plane, member_rows(member), columns(c)],
+            dst_ref=arrived.at[plane, member_rows(q), columns(c)],
+            send_sem=fsend.at[plane], recv_sem=frecv.at[plane],
+            device_id=place(z, member), device_id_type=MESH_ID,
+        )
+
+    def backward(plane, c, member):
+        return pltpu.make_async_remote_copy(
+            src_ref=done.at[plane, member_rows(member), columns(c)],
+            dst_ref=back.at[plane, member_rows(q), columns(c)],
+            send_sem=bsend.at[plane], recv_sem=brecv.at[plane, c],
+            device_id=place(z, member), device_id_type=MESH_ID,
+        )
+
+    def home(plane, c):
+        return pltpu.make_async_remote_copy(
+            src_ref=part.at[plane, :, columns(c)], dst_ref=parts.at[z, :, columns(c)],
+            send_sem=psend.at[plane, c], recv_sem=precv.at[z, c],
+            device_id=place(plane, q), device_id_type=MESH_ID,
+        )
+
+    def homed(plane, c):
+        return pltpu.make_async_copy(
+            parts.at[plane, :, columns(c)], parts.at[plane, :, columns(c)], precv.at[plane, c]
+        )
+
+    others = pl.ds(0, (per - 1) * cap)
+
+    def whole(ref, plane, sem):
+        view = ref.at[plane, others, :]
+        return pltpu.make_async_copy(view, view, sem.at[plane])
+
+    def slab(plane, c):
+        view = back.at[plane, others, columns(c)]
+        return pltpu.make_async_copy(view, view, brecv.at[plane, c])
+
+    line[z] = ffn_ref[...]
+    ids = ids_ref[...]
+    group_size = experts // EXPERT_GROUPS
+    weight = jnp.zeros(ids.shape, jnp.float32)
+    for g in range(EXPERT_GROUPS):
+        inside = (ids >= g * group_size) & (ids < (g + 1) * group_size)
+        weight = weight + jnp.where(inside, group_ref[g : g + 1, :], 0.0)
+    choose = ids.shape[0]
+    info = jnp.concatenate(
+        [
+            ids.astype(jnp.float32), weight * weight_ref[...],
+            jnp.zeros((meta.shape[1] - 2 * choose, rows), jnp.float32),
+        ],
+        axis=0,
+    )
+    meta[z] = info
+    pl.semaphore_wait(barrier, per + planes - 2)
+    loop(1, planes, lambda d: tell(z, (z + d) % planes).start())
+    for c in range(chunks):
+        @pl.when(z < planes - 1)
+        def _():
+            hop(z, c, 1).start()
+
+        @pl.when(z > 0)
+        def _():
+            hop(z, c, 0).start()
+
+    slot_member = lax.broadcasted_iota(jnp.int32, (per, cap, rows), 0).reshape(rows, rows)
+    slot_place = lax.broadcasted_iota(jnp.int32, (per, cap, rows), 1).reshape(rows, rows)
+    slot_expert = (slot_member + z * per).astype(jnp.float32)
+    slot_place = slot_place.astype(jnp.float32)
+    earlier = (
+        lax.broadcasted_iota(jnp.int32, (rows, rows), 0)
+        < lax.broadcasted_iota(jnp.int32, (rows, rows), 1)
+    ).astype(jnp.bfloat16)
+
+    def sort_out(plane):
+        known = meta[plane]
+        named = jnp.zeros((rows, rows), jnp.float32)
+        value = jnp.zeros((rows, rows), jnp.float32)
+        for k in range(choose):
+            chosen = (known[k : k + 1, :] == slot_expert).astype(jnp.float32)
+            named = named + chosen
+            value = value + chosen * known[choose + k : choose + k + 1, :]
+        rank = jnp.dot(named.astype(jnp.bfloat16), earlier, preferred_element_type=jnp.float32)
+        hot = jnp.where(rank == slot_place, named, 0.0)
+        picks[plane] = hot.astype(jnp.bfloat16)
+        routes[plane] = jnp.transpose(hot * value).astype(jnp.bfloat16)
+
+    lag = chunks + 2
+
+    def stage_rows(k, c, up, plane):
+        @pl.when(k > 0)
+        def _():
+            hop(plane, c, up).wait_recv()
+
+            @pl.when((up == 0) & (z < planes - 1))
+            def _():
+                hop(plane, c, 1).start()
+
+            @pl.when((up == 1) & (z > 0))
+            def _():
+                hop(plane, c, 0).start()
+
+        @pl.when(c == 0)
+        def _():
+            @pl.when(k > 0)
+            def _():
+                tell(plane, plane).wait_recv()
+
+            sort_out(plane)
+
+        at = columns(c)
+        slots[plane, :, at] = jnp.dot(
+            picks[plane], line[plane, :, at], preferred_element_type=jnp.float32
+        ).astype(jnp.bfloat16)
+        arrived[plane, member_rows(q), at] = slots[plane, member_rows(q), at]
+        loop(1, per, lambda d: forward(plane, c, (q + d) % per).start())
+
+    def stage_experts(k, plane):
+        @pl.when(k == 0)
+        def _():
+            for load in loads:
+                load.wait()
+
+        whole(arrived, plane, frecv).wait()
+        tokens = arrived[plane]
         gate = jnp.dot(tokens, wg[...], preferred_element_type=jnp.float32)
         up = jnp.dot(tokens, wu[...], preferred_element_type=jnp.float32)
         hidden = (silu(gate) * up).astype(jnp.bfloat16)
-        for j in range(model // piece):
-            at = slice(j * piece, (j + 1) * piece)
-            done[part, at] = jnp.dot(
+        for c in range(chunks):
+            at = slice(c * width, (c + 1) * width)
+            done[plane, :, at] = jnp.dot(
                 hidden, wd[:, at], preferred_element_type=jnp.float32
             ).astype(jnp.bfloat16)
-        loop(max(low, 1), low + size, lambda k: backward(k).start())
-    mine = pltpu.make_async_copy(done.at[rows(0), :], back.at[rows(me), :], local.at[1])
-    mine.start()
-    mine.wait()
-    loop(1, n, lambda k: forward(k).wait_send())
-    loop(1, n, lambda k: returned(k).wait_recv())
-    for j in range(model // piece):
-        at = slice(j * piece, (j + 1) * piece)
-        total = mixed_ref[:, at].astype(jnp.float32)
-        total += jnp.dot(high_ref[...], back[:, at], preferred_element_type=jnp.float32)
-        total += jnp.dot(low_ref[...], back[:, at], preferred_element_type=jnp.float32)
-        out_ref[:, at] = total.astype(jnp.bfloat16)
-    loop(1, n, lambda k: backward(k).wait_send())
-
-
-def exchange(ffn, pick, high, low, mixed, gate_weight, up_weight, down_weight):
-    n = lax.axis_size("sp") * lax.axis_size("tp")
-    slots, model = pick.shape[0], ffn.shape[1]
-    bf = jnp.bfloat16
+            back[plane, member_rows(q), at] = done[plane, member_rows(q), at]
+            loop(1, per, lambda d: backward(plane, c, (q + d) % per).start())
+
+    def stage_home(k, c, plane):
+        slab(plane, c).wait()
+        at = columns(c)
+        total = jnp.dot(
+            routes[plane], back[plane, :, at], preferred_element_type=jnp.float32
+        )
+
+        @pl.when(k == 0)
+        def _():
+            mine[:, at] = total
+
+        @pl.when(k > 0)
+        def _():
+            part[plane, :, at] = total.astype(jnp.bfloat16)
+            home(plane, c).start()
+
+    def tick(v):
+        def both(k, act):
+            def side(up):
+                plane = z + k * (2 * up - 1)
+
+                @pl.when((plane >= 0) & (plane < planes) & ((k > 0) | (up == 0)))
+                def _():
+                    act(up, plane)
+
+            loop(0, 2, side)
+
+        @pl.when(v < planes * chunks)
+        def _():
+            k = v // chunks
+            c = v % chunks
+            both(k, lambda up, plane: stage_rows(k, c, up, plane))
+
+        @pl.when((v % chunks == 0) & (v >= chunks) & (v <= planes * chunks))
+        def _():
+            k = v // chunks - 1
+            both(k, lambda up, plane: stage_experts(k, plane))
+
+        @pl.when(v >= lag)
+        def _():
+            k = (v - lag) // chunks
+            c = (v - lag) % chunks
+            both(k, lambda up, plane: stage_home(k, c, plane))
+
+    loop(0, planes * chunks + lag, tick)
+
+    for c in range(chunks):
+        at = slice(c * width, (c + 1) * width)
+        loop(1, planes, lambda d: homed((z + d) % planes, c).wait())
+        mine[:, at] = mine[:, at] + mixed_ref[:, at].astype(jnp.float32)
+
+        def add(d):
+            mine[:, at] = mine[:, at] + parts[(z + d) % planes, :, at].astype(jnp.float32)
+
+        loop(1, planes, add)
+        out_ref[:, at] = mine[:, at].astype(jnp.bfloat16)
+
+    loop(1, planes, lambda d: tell(z, (z + d) % planes).wait_send())
+
+    def finish(plane):
+        whole(slots, plane, fsend).wait()
+        whole(done, plane, bsend).wait()
+
+        def each(c):
+            @pl.when((plane <= z) & (z < planes - 1))
+            def _():
+                hop(plane, c, 1).wait_send()
+
+            @pl.when((plane >= z) & (z > 0))
+            def _():
+                hop(plane, c, 0).wait_send()
+
+            @pl.when(plane != z)
+            def _():
+                home(plane, c).wait_send()
+
+        loop(0, chunks, each)
+
+    loop(0, planes, finish)
+
+
+def exchange(ffn, ids, group_weight, chosen_weight, mixed, gate_weight, up_weight, down_weight,
+             planes):
+    rows, model = ffn.shape
+    chunks = 4
+    bf, f32 = jnp.bfloat16, jnp.float32
     vm = pltpu.VMEM
+    dma = pltpu.SemaphoreType.DMA
     return pl.pallas_call(
-        functools.partial(expert_kernel, n, lax.axis_size("tp")),
+        functools.partial(plane_kernel, planes, lax.axis_size("tp")),
         out_shape=jax.ShapeDtypeStruct(mixed.shape, bf),
         in_specs=[pl.BlockSpec(memory_space=pltpu.VMEM)] * 5
         + [pl.BlockSpec(memory_space=pl.ANY)] * 3,
@@ -454,16 +632,21 @@
         scratch_shapes=[
             vm(gate_weight.shape[1:], bf), vm(up_weight.shape[1:], bf),
             vm(down_weight.shape[1:], bf),
-            vm((slots, model), bf), vm((slots, model), bf), vm((slots, model), bf),
-            vm((slots, model), bf),
-            pltpu.SemaphoreType.DMA((3,)), pltpu.SemaphoreType.DMA((2,)),
-            pltpu.SemaphoreType.DMA((n,)), pltpu.SemaphoreType.DMA((n,)),
-            pltpu.SemaphoreType.DMA((n,)), pltpu.SemaphoreType.DMA((n,)),
+            vm((planes, 8, rows), f32),
+            vm((planes, rows, rows), bf), vm((planes, rows, rows), bf),
+            vm((planes, rows, model), bf), vm((planes, rows, model), bf),
+            vm((planes, rows, model), bf), vm((planes, rows, model), bf),
+            vm((planes, rows, model), bf), vm((planes, rows, model), bf),
+            vm((rows, model), f32), vm((planes, rows, model), bf),
+            dma((3,)), dma((planes,)), dma((planes,)),
+            dma((2, planes, chunks)), dma((planes, chunks)),
+            dma((planes,)), dma((planes,)), dma((planes,)), dma((planes, chunks)),
+            dma((planes, chunks)), dma((planes, chunks)),
         ],
         compiler_params=pltpu.CompilerParams(
             collective_id=1, has_side_effects=True, vmem_limit_bytes=56 * 1024 * 1024
         ),
-    )(ffn, pick, high, low, mixed, gate_weight, up_weight, down_weight)
+    )(ffn, ids, group_weight, chosen_weight, mixed, gate_weight, up_weight, down_weight)
 
 
 def local(
@@ -500,6 +683,15 @@
     row_count, width = ffn_in.shape
     choose = chosen_expert_index.shape[1]
     capacity = 2 * mixer_value_rows.shape[0] // experts
+    per = row_count // capacity
+    if (
+        capacity % 16 == 0 and row_count % capacity == 0 and experts % per == 0
+        and per % lax.axis_size("tp") == 0 and experts % EXPERT_GROUPS == 0 and choose <= 4
+    ):
+        return exchange(
+            ffn_in, chosen_expert_index.T, expert_group_weight.T, chosen_expert_weight.T,
+            mixed_rows, expert_gate_weight, expert_up_weight, expert_down_weight, experts // per,
+        )
     ids = jnp.arange(experts, dtype=jnp.int32)
     chosen = (chosen_expert_index[:, :, None] == ids).astype(jnp.bfloat16)
     named = jnp.sum(chosen, axis=1)
@@ -516,11 +708,6 @@
     route = jnp.where(hot, weight[:, :, None], 0.0).reshape(row_count, experts * capacity)
     route_high = route.astype(jnp.bfloat16)
     route_low = (route - route_high.astype(jnp.float32)).astype(jnp.bfloat16)
-    if capacity % 16 == 0 and experts % 4 == 0:
-        return exchange(
-            ffn_in, pick.T, route_high, route_low, mixed_rows,
-            expert_gate_weight, expert_up_weight, expert_down_weight,
-        )
     outgoing = lax.dot_general(
         pick, ffn_in, (((0,), (0,)), ((), ())), preferred_element_type=jnp.float32
     ).astype(jnp.bfloat16)

time: 174 us -> 151 us (0.87)
  Pallas kernels: 159 us -> 142 us
  other arithmetic: 4.29 us -> 0.68 us
    pallas_call x1, Pallas kernels: 128 us -> 110 us  [exchange(): pl.pallas_call(functools.partial(plane_kernel, planes, lax.axis_size('tp'...]
    reduce_sum x3 -> x0, other arithmetic: 2.17 us -> none  [the longest x1 0.78 us: local(): jnp.sum(expert_group_weight[:, :, None] * group_of[None], axis=1)]
where the time goes in v1:
time: 151 us; the launch traced here: 150 us
  Pallas kernels  142 us (94%)
  local copies, waits for them, and re-layouts  7.56 us (5%)
    pallas_call x1, Pallas kernels, exchange(): pl.pallas_call(functools.partial(plane_kernel, planes, lax.axis_size('tp'...  110 us
    pallas_call x1, Pallas kernels, mixer(): pl.pallas_call(functools.partial(mixer_kernel, n), out_shape=[jax.ShapeDt...  31.7 us
    unnamed x3, local copies, waits for them, and re-layouts  4.82 us

profile of v1, /device:TPU:0, one launch (start us, length us, event | category | flops | bytes accessed | tf_op | source)
XLA Modules:
  0.0 150.3 jit_solution(16158519330459058630)
XLA Ops:
  0.0 0.7 add_convert_fusion
  0.7 0.6 broadcast_in_dim.27.docrow_ref
  1.3 0.7 broadcast_in_dim.26
  2.0 0.7 broadcast_in_dim_reshape.3.direct_ref
  2.7 0.8 broadcast_in_dim.24.docs_hbm
  3.4 1.5 copy.24.step_hbm
  4.9 1.5 copy.25.extra_hbm
  6.4 31.7 %shard_map.217 = (bf16[128,2048]{1,0:T(8,128)(2,1)}, bf16[128,2048]{1,0:T(8,128)(2,1)}) custom-call(bf16[256,1024]{1,0:T(8,128)(2,1)} %x_hbm.1, bf16[256,128]{1,0:T(8,128)(2,1)} %b_hbm.1, bf16[256,128]{1,0:T(8,128)(2,1)} %c_hbm.1, bf16[256,1024]{1,0:T(8,128)(2,1)} %gate_hbm.1, f32[256,16]{1,0:T(8,128)} %copy.24.step_hbm, f32[256,16]{1,0:T(8,128)} %copy.25.extra_hbm, ...), custom_call_target="tpu_custom_call" | custom-call | tf_op jit(solution)/shard_map/pallas_call | solution.py:307
  38.0 110.4 %shard_map.218 = bf16[128,2048]{1,0:T(8,128)(2,1)} custom-call(bf16[128,2048]{1,0:T(8,128)(2,1)} %get-tuple-element.7.ffn_ref, s32[2,128]{1,0:T(2,128)} %bitcast.9, f32[4,128]{1,0:T(4,128)} %bitcast.8, f32[2,128]{1,0:T(2,128)} %bitcast.10, bf16[128,2048]{1,0:T(8,128)(2,1)} %get-tuple-element.8.mixed_ref, bf16[1,2048,512]{2,1,0:T(8,128)(2,1)} %wg_hbm.1, ...), custom_call_target="tpu_custom_call" | custom-call | tf_op jit(solution)/shard_map/pallas_call | solution.py:626
  148.4 1.9 %copy.27 = bf16[128,2048]{1,0:T(8,128)(2,1)} copy(bf16[128,2048]{1,0:T(8,128)(2,1)} %shard_map.218) | data formatting | bytes 1048576

commit v2 on v1

--- a/solution.py
+++ b/solution.py
@@ -15,7 +15,7 @@
 
 NEG = -1e30
 MESH_ID = pl.DeviceIdType.MESH
-OFFSETS = (1, 2, 5)
+HOSTS = 4
 
 
 def softplus(v):
@@ -31,13 +31,14 @@
 
 
 def mixer_kernel(
-    n, x_hbm, b_hbm, c_hbm, gate_hbm, step_hbm, extra_hbm, docs_hbm, resid_hbm, w_hbm,
-    rate_ref, direct_ref, spread_ref, taps_ref, btaps_ref, ctaps_ref, docrow_ref, gain_ref,
-    gain2_ref,
+    n, x_hbm, b_hbm, c_hbm, gate_hbm, resid_hbm, w_hbm,
+    step_ref, extra_ref, docrow_ref, rate_ref, direct_ref, taps_ref, btaps_ref, ctaps_ref,
+    gain_ref, gain2_ref,
     mixed_ref, ffn_ref,
-    x_ref, b_ref, c_ref, gate_ref, step_ref, extra_ref, docs_ref, resid_ref, w_ref, pad, pad_docs, edge_x, edge_b, edge_c, edge_d,
-    vconv, bconv, cconv, ylocal, cumx, s32, t0, t1, t2, g0, g1, g2,
-    r0, r1, r1far, r2, rg0, rg1, rg2, gated, regrouped,
+    x_ref, b_ref, c_ref, gate_ref, resid_ref, w_ref, docs_ref, pad, pad_docs,
+    edge_x, edge_b, edge_c, edge_d,
+    vconv, bconv, cconv, ylocal, cumx, t0, g0, rs, rg, tot, grow, rt, rgrow, hs, incoming,
+    gated, regrouped,
     wsem, send, recv,
 ):
     sp = lax.axis_index("sp")
@@ -46,25 +47,34 @@
     state = b_ref.shape[1]
     lanes = 128
     chunks = channels // lanes
-    heads = step_ref.shape[1]
+    heads = step_ref.shape[0]
     half = length // 2
     edge = edge_x.shape[0]
+    hosts, _, block = rs.shape
+    member = sp % hosts
+    base_sp = sp - member
 
     loads = [
         pltpu.make_async_copy(source, target, wsem.at[i])
         for i, (source, target) in enumerate((
-            (x_hbm, x_ref), (b_hbm, b_ref), (c_hbm, c_ref), (docs_hbm, docs_ref),
-            (step_hbm, step_ref), (extra_hbm, extra_ref), (gate_hbm, gate_ref),
+            (x_hbm, x_ref), (b_hbm, b_ref), (c_hbm, c_ref), (gate_hbm, gate_ref),
             (resid_hbm, resid_ref), (w_hbm, w_ref),
         ))
     ]
     for load in loads:
         load.start()
 
+    docs_row = docrow_ref[...].astype(jnp.float32) + 1.0
+    docs_ref[...] = jnp.transpose(jnp.broadcast_to(docs_row, (lanes, length)))
+
     barrier = pltpu.get_barrier_semaphore()
-    count = jnp.int32(1)
+    count = jnp.int32(hosts)
     pl.semaphore_signal(barrier, inc=1, device_id=(sp, 1 - tp), device_id_type=MESH_ID)
-    for off in OFFSETS:
+    for d in range(1, hosts):
+        pl.semaphore_signal(
+            barrier, inc=1, device_id=(base_sp + (member + d) % hosts, tp), device_id_type=MESH_ID
+        )
+    for off in (1, hosts, 2 * hosts):
         @pl.when(sp + off < n)
         def _():
             pl.semaphore_signal(barrier, inc=1, device_id=(sp + off, tp), device_id_type=MESH_ID)
@@ -76,11 +86,33 @@
         count = count + (sp + off < n).astype(jnp.int32) + (sp >= off).astype(jnp.int32)
     pl.semaphore_wait(barrier, count)
 
+    def remote(sent, received, src, dst, device):
+        return pltpu.make_async_remote_copy(
+            src_ref=src, dst_ref=dst, send_sem=send.at[sent], recv_sem=recv.at[received],
+            device_id=(device, tp), device_id_type=MESH_ID,
+        )
+
     def copy(slot, src, dst, off):
-        return pltpu.make_async_remote_copy(
-            src_ref=src, dst_ref=dst, send_sem=send.at[slot], recv_sem=recv.at[slot],
-            device_id=(sp + off, tp), device_id_type=MESH_ID,
-        )
+        return remote(slot, slot, src, dst, sp + off)
+
+    def part_of(i):
+        return pl.ds(pl.multiple_of(i * block, block), block)
+
+    def give(i, source):
+        return [
+            remote(4 + i, 4 + source, t0.at[:, part_of(i)], rs.at[source], base_sp + i),
+            remote(
+                4 + hosts + i, 4 + hosts + source, g0.at[:, part_of(i)], rg.at[source], base_sp + i
+            ),
+        ]
+
+    def enter(i, source):
+        return remote(
+            4 + 2 * hosts + i, 4 + 2 * hosts + source, hs.at[i], incoming.at[:, part_of(source)],
+            base_sp + i,
+        )
+
+    others = [(member + d) % hosts for d in range(1, hosts)]
 
     last = pl.ds(length - edge, edge)
     edges = [
@@ -108,23 +140,28 @@
             for one in copies:
                 one.wait_send()
 
-    for load in loads[:4]:
+    for load in loads[:3]:
         load.wait()
     start(edges, 1)
-    for load in loads[4:6]:
-        load.wait()
-
+
+    head_row = lax.broadcasted_iota(jnp.int32, (heads, heads), 0)
+    head_col = lax.broadcasted_iota(jnp.int32, (heads, heads), 1)
+
+    def column(ref):
+        return jnp.sum(jnp.where(head_row == head_col, ref[...], 0.0), axis=1, keepdims=True)
+
+    direct_column = column(direct_ref)
     step = softplus(step_ref[...])
-    logs = extra_ref[...] - step * rate_ref[...]
+    logs = extra_ref[...] - step * column(rate_ref)
     rows = lax.broadcasted_iota(jnp.int32, (length, length), 0)
     cols = lax.broadcasted_iota(jnp.int32, (length, length), 1)
     causal = rows >= cols
-    cum = exact_dot(causal.astype(jnp.float32), logs)
-    cum_t = lax.dot_general(
-        logs, (rows <= cols).astype(jnp.float32), (((0,), (0,)), ((), ())),
+    cum = lax.dot_general(
+        causal.astype(jnp.float32), logs, (((1,), (1,)), ((), ())),
         preferred_element_type=jnp.float32, precision=lax.Precision.HIGHEST,
     )
-    same = docs_ref[:, 0:1] == docrow_ref[0:1, :]
+    cum_t = exact_dot(logs, (rows <= cols).astype(jnp.float32))
+    same = docs_ref[:, 0:1] == docs_row
     blocked = jnp.where(causal & same, 0.0, NEG)
     tail = (docs_ref[...] == docs_ref[length - 1 : length, :]).astype(jnp.float32)
 
@@ -165,31 +202,49 @@
     keep = (docs_ref[length - 1 : length, :] == pad_docs[edge - 1 : edge, :]).astype(jnp.float32)
     keep = keep * has.astype(jnp.float32)
     b_t = jnp.transpose(bconv[...].astype(jnp.float32)).astype(jnp.bfloat16)
+    per_chunk = heads // chunks
+    width = lanes // per_chunk
+    spread_row = lax.broadcasted_iota(jnp.int32, (heads, lanes), 0) * width
+    spread_lane = lax.broadcasted_iota(jnp.int32, (heads, lanes), 1)
+
+    def widen(j):
+        at = spread_lane + j * lanes - spread_row
+        return jnp.where((at >= 0) & (at < width), 1.0, 0.0)
+
     for j in range(chunks):
         at = slice(j * lanes, (j + 1) * lanes)
         value = conv(j * lanes, taps_ref, j * lanes)
         vconv[:, at] = value
-        widen = spread_ref[:, at]
-        cum_wide = exact_dot(cum, widen)
+        wide = widen(j)
+        cum_wide = exact_dot(cum, wide)
         cumx[:, at] = cum_wide
-        stepped = (exact_dot(step, widen) * value.astype(jnp.float32)).astype(jnp.bfloat16)
+        step_wide = lax.dot_general(
+            step, wide, (((0,), (0,)), ((), ())),
+            preferred_element_type=jnp.float32, precision=lax.Precision.HIGHEST,
+        )
+        stepped = (step_wide * value.astype(jnp.float32)).astype(jnp.bfloat16)
         ylocal[:, at] = stepped.astype(jnp.float32)
         ending = cum_wide[length - 1 : length, :]
         ended = (jnp.exp(ending - cum_wide) * tail * stepped.astype(jnp.float32)).astype(
             jnp.bfloat16
         )
-        fresh = jnp.dot(b_t, ended, preferred_element_type=jnp.float32)
-        s32[:, at] = fresh
-        t0[:, at] = fresh.astype(jnp.bfloat16)
+        t0[:, at] = jnp.dot(b_t, ended, preferred_element_type=jnp.float32).astype(jnp.bfloat16)
         g0[:, at] = jnp.broadcast_to(jnp.exp(ending) * keep, (8, lanes))
-    first = [copy(4, t0, r0, 1), copy(5, g0, rg0, 1)]
-    start(first, 1)
+        i = j * lanes // block
+        if (j + 1) * lanes == (i + 1) * block:
+            @pl.when(member != i)
+            def _():
+                for one in give(i, member):
+                    one.start()
+
+            @pl.when(member == i)
+            def _():
+                rs[i] = t0[:, i * block : (i + 1) * block]
+                rg[i] = g0[:, i * block : (i + 1) * block]
 
     scores = lax.dot_general(
         cconv[...], bconv[...], (((1,), (1,)), ((), ())), preferred_element_type=jnp.float32
     )
-    per_chunk = heads // chunks
-    width = lanes // per_chunk
     lane = lax.broadcasted_iota(jnp.int32, (length, lanes), 1)
 
     def inside(j):
@@ -203,44 +258,55 @@
                 (scores * decay).astype(jnp.bfloat16), stepped, preferred_element_type=jnp.float32
             )
             result = part if result is None else jnp.where(lane < k * width, result, part)
-        direct = direct_ref[:, at]
+        direct = jnp.sum(widen(j) * direct_column, axis=0, keepdims=True)
         ylocal[:, at] = result + direct * vconv[:, at].astype(jnp.float32)
 
-    third = chunks // 3
-    for j in range(third):
+    early = chunks // 4
+    late = chunks * 5 // 8
+    for j in range(early):
         inside(j)
 
-    wait_recv(first, 1)
-    grow0 = g0[0:1, :]
-    before = jnp.where(has, r0[...].astype(jnp.float32), 0.0)
-    s32[...] = s32[...] + grow0 * before
-    t1[...] = s32[...].astype(jnp.bfloat16)
-    g1[...] = g0[...] * jnp.where(has, rg0[...], 0.0)
-    second = [copy(6, t1, r1, 2), copy(7, g1, rg1, 2)]
-    far = [copy(8, t1, r1far, 5)]
-    start(second, 2)
-    start(far, 5)
-    for j in range(third, 2 * third):
+    for i in others:
+        for one in give(i, i):
+            one.wait_recv()
+    total = jnp.zeros((state, block), jnp.float32)
+    growth = jnp.ones((1, block), jnp.float32)
+    for i in range(hosts):
+        factor = rg[i][0:1, :]
+        total = rs[i].astype(jnp.float32) + factor * total
+        growth = growth * factor
+    tot[...] = total.astype(jnp.bfloat16)
+    grow[...] = jnp.broadcast_to(growth, grow.shape)
+    slot = 4 + 3 * hosts
+    nearer = [copy(slot, tot, rt.at[0], hosts), copy(slot + 1, grow, rgrow, hosts)]
+    further = [copy(slot + 2, tot, rt.at[1], 2 * hosts)]
+    start(nearer, hosts)
+    start(further, 2 * hosts)
+    for j in range(early, late):
         inside(j)
 
-    wait_recv(second, 2)
-    has2 = sp >= 2
-    before = jnp.where(has2, r1[...].astype(jnp.float32), 0.0)
-    t2[...] = (s32[...] + g1[0:1, :] * before).astype(jnp.bfloat16)
-    g2[...] = g1[...] * jnp.where(has2, rg1[...], 0.0)
-    final = [copy(9, t2, r2, 1), copy(10, g2, rg2, 1)]
-    start(final, 1)
-    for j in range(2 * third, chunks):
+    wait_recv(nearer, hosts)
+    wait_recv(further, 2 * hosts)
+    carried = jnp.where(sp >= 2 * hosts, rt[1].astype(jnp.float32), 0.0)
+    carried = jnp.where(sp >= hosts, rt[0].astype(jnp.float32) + rgrow[0:1, :] * carried, 0.0)
+    for i in range(hosts):
+        @pl.when(member != i)
+        def _():
+            hs[i] = carried.astype(jnp.bfloat16)
+            enter(i, member).start()
+
+        @pl.when(member == i)
+        def _():
+            incoming[:, i * block : (i + 1) * block] = carried.astype(jnp.bfloat16)
+
+        if i < hosts - 1:
+            carried = rs[i].astype(jnp.float32) + rg[i][0:1, :] * carried
+    for j in range(late, chunks):
         inside(j)
 
-    wait_recv(final, 1)
-    wait_recv(far, 5)
-    has5 = sp >= 5
-    incoming = (
-        jnp.where(has, r2[...].astype(jnp.float32), 0.0)
-        + jnp.where(has, rg2[0:1, :], 0.0) * jnp.where(has5, r1far[...].astype(jnp.float32), 0.0)
-    ).astype(jnp.bfloat16)
-    loads[6].wait()
+    for i in others:
+        enter(i, i).wait_recv()
+    loads[3].wait()
     entering = (docs_ref[...] == pad_docs[edge - 1 : edge, :]).astype(jnp.float32)
     for j in range(chunks):
         at = slice(j * lanes, (j + 1) * lanes)
@@ -251,17 +317,19 @@
     swap = pltpu.make_async_remote_copy(
         src_ref=gated.at[pl.ds(pl.multiple_of((1 - tp) * half, half), half), :],
         dst_ref=regrouped,
-        send_sem=send.at[11], recv_sem=recv.at[11],
+        send_sem=send.at[slot + 3], recv_sem=recv.at[slot + 3],
         device_id=(sp, 1 - tp), device_id_type=MESH_ID,
     )
     swap.start()
     wait_send(edges, 1)
-    wait_send(first, 1)
-    wait_send(second, 2)
-    wait_send(far, 5)
-    wait_send(final, 1)
-    loads[7].wait()
-    loads[8].wait()
+    wait_send(nearer, hosts)
+    wait_send(further, 2 * hosts)
+    for i in others:
+        for one in give(i, member):
+            one.wait_send()
+        enter(i, member).wait_send()
+    loads[4].wait()
+    loads[5].wait()
     swap.wait()
     own = gated[pl.ds(pl.multiple_of(tp * half, half), half), :].astype(jnp.float32)
     other = regrouped[...].astype(jnp.float32)
@@ -291,48 +359,43 @@
           weight, gain2):
     length, channels = x.shape
     state = b.shape[1]
-    heads = step.shape[1]
-    width = channels // heads
-    model = resid.shape[1]
-    half = resid.shape[0]
-    assert state == D_STATE and (LONGEST - 2) // length + 1 <= 6
-    marks = (docs + 1).astype(jnp.float32)
-    docs_wide = jnp.broadcast_to(marks[:, None], (length, 128))
-    docs_row = jnp.broadcast_to(marks[None, :], (8, length))
-    spread = jnp.asarray(np.repeat(np.eye(heads, dtype=np.float32), width, axis=1))
-    direct_wide = jnp.repeat(direct, width)[None, :]
+    half, model = resid.shape
+    hosts = HOSTS
+    block = channels // hosts
+    assert state == D_STATE and n % hosts == 0 and block % 128 == 0
+    assert (LONGEST - 2) // (hosts * length) + 1 <= 2
     bf, f32 = jnp.bfloat16, jnp.float32
     edge = 16
     vm = pltpu.VMEM
+    sems = 4 + 3 * hosts + 4
     return pl.pallas_call(
         functools.partial(mixer_kernel, n),
         out_shape=[jax.ShapeDtypeStruct((half, model), bf)] * 2,
-        in_specs=[pl.BlockSpec(memory_space=pl.ANY)] * 9
-        + [pl.BlockSpec(memory_space=pltpu.VMEM)] * 9,
+        in_specs=[pl.BlockSpec(memory_space=pl.ANY)] * 6
+        + [pl.BlockSpec(memory_space=pltpu.VMEM)] * 10,
         out_specs=[pl.BlockSpec(memory_space=pltpu.VMEM)] * 2,
         scratch_shapes=[
             vm(x.shape, bf), vm(b.shape, bf), vm(c.shape, bf), vm(gate.shape, bf),
-            vm(step.shape, f32), vm(extra.shape, f32), vm(docs_wide.shape, f32),
-            vm(resid.shape, bf), vm(weight.shape, bf),
+            vm(resid.shape, bf), vm(weight.shape, bf), vm((length, 128), f32),
             vm((edge + length, channels + 2 * state), f32), vm((edge + length, 128), f32),
             vm((edge, channels), bf), vm((edge, state), bf), vm((edge, state), bf),
             vm((edge, 128), f32),
             vm((length, channels), bf), vm((length, state), bf), vm((length, state), bf),
             vm((length, channels), f32), vm((length, channels), f32),
-            vm((state, channels), f32),
-            vm((state, channels), bf), vm((state, channels), bf), vm((state, channels), bf),
-            vm((8, channels), f32), vm((8, channels), f32), vm((8, channels), f32),
-            vm((state, channels), bf), vm((state, channels), bf), vm((state, channels), bf),
-            vm((state, channels), bf),
-            vm((8, channels), f32), vm((8, channels), f32), vm((8, channels), f32),
+            vm((state, channels), bf), vm((8, channels), f32),
+            vm((hosts, state, block), bf), vm((hosts, 8, block), f32),
+            vm((state, block), bf), vm((8, block), f32),
+            vm((2, state, block), bf), vm((8, block), f32),
+            vm((hosts, state, block), bf), vm((state, channels), bf),
             vm((length, channels), bf), vm((half, channels), bf),
-            pltpu.SemaphoreType.DMA((9,)), pltpu.SemaphoreType.DMA((12,)), pltpu.SemaphoreType.DMA((12,)),
+            pltpu.SemaphoreType.DMA((6,)), pltpu.SemaphoreType.DMA((sems,)),
+            pltpu.SemaphoreType.DMA((sems,)),
         ],
         compiler_params=pltpu.CompilerParams(
             collective_id=0, has_side_effects=True, vmem_limit_bytes=58 * 1024 * 1024
         ),
-    )(x, b, c, gate, step, extra, docs_wide, resid, weight, rate[None, :], direct_wide, spread,
-      taps, btaps, ctaps, docs_row, gain[None, :], gain2[None, :])
+    )(x, b, c, gate, resid, weight, step.T, extra.T, docs[None, :], rate[None, :], direct[None, :],
+      taps, btaps, ctaps, gain[None, :], gain2[None, :])
 
 
 def plane_kernel(

time: 151 us -> 124 us (0.82)
  Pallas kernels: 142 us -> 122 us
  local copies, waits for them, and re-layouts: 7.56 us -> 1.88 us
    pallas_call x1, Pallas kernels: 110 us -> 96.3 us  [exchange(): pl.pallas_call(functools.partial(plane_kernel, planes, lax.axis_size('tp'...]
    pallas_call x1, Pallas kernels: 31.7 us -> 25.8 us  [mixer(): pl.pallas_call(functools.partial(mixer_kernel, n), out_shape=[jax.ShapeDt...]
    unnamed x3 -> x1, local copies, waits for them, and re-layouts: 4.82 us -> 1.88 us
    broadcast_in_dim x3 -> x0, local copies, waits for them, and re-layouts: 2.08 us -> none  [the longest x1 0.76 us: mixer(): docs_wide = jnp.broadcast_to(marks[:, None], (length, 128))]
where the time goes in v2:
time: 124 us
  Pallas kernels  122 us (98%)
  local copies, waits for them, and re-layouts  1.88 us (2%)
    pallas_call x1, Pallas kernels, exchange(): pl.pallas_call(functools.partial(plane_kernel, planes, lax.axis_size('tp'...  96.3 us
    pallas_call x1, Pallas kernels, mixer(): pl.pallas_call(functools.partial(mixer_kernel, n), out_shape=[jax.ShapeDt...  25.8 us

profile of v2, /device:TPU:0, one launch (start us, length us, event | category | flops | bytes accessed | tf_op | source)
XLA Modules:
  0.0 124.0 jit_solution(10136176443170378929)
XLA Ops:
  0.0 25.8 %shard_map.208 = (bf16[128,2048]{1,0:T(8,128)(2,1)}, bf16[128,2048]{1,0:T(8,128)(2,1)}) custom-call(bf16[256,1024]{1,0:T(8,128)(2,1)} %x_hbm.1, bf16[256,128]{1,0:T(8,128)(2,1)} %b_hbm.1, bf16[256,128]{1,0:T(8,128)(2,1)} %c_hbm.1, bf16[256,1024]{1,0:T(8,128)(2,1)} %gate_hbm.1, bf16[128,2048]{1,0:T(8,128)(2,1)} %resid_hbm.1, bf16[2048,2048]{1,0:T(8,128)(2,1)} %w_hbm.1, ...), custom_call_target="tpu_custom_call" | custom-call | tf_op jit(solution)/shard_map/pallas_call | solution.py:371
  25.8 96.3 %shard_map.209 = bf16[128,2048]{1,0:T(8,128)(2,1)} custom-call(bf16[128,2048]{1,0:T(8,128)(2,1)} %get-tuple-element.7.ffn_ref, s32[2,128]{1,0:T(2,128)} %bitcast.15, f32[4,128]{1,0:T(4,128)} %bitcast.14, f32[2,128]{1,0:T(2,128)} %bitcast.16, bf16[128,2048]{1,0:T(8,128)(2,1)} %get-tuple-element.8.mixed_ref, bf16[1,2048,512]{2,1,0:T(8,128)(2,1)} %wg_hbm.1, ...), custom_call_target="tpu_custom_call" | custom-call | tf_op jit(solution)/shard_map/pallas_call | solution.py:689
  122.1 1.9 %copy.24 = bf16[128,2048]{1,0:T(8,128)(2,1)} copy(bf16[128,2048]{1,0:T(8,128)(2,1)} %shard_map.209) | data formatting | bytes 1048576

commit v3 on v2

--- a/solution.py
+++ b/solution.py
@@ -31,7 +31,7 @@
 
 
 def mixer_kernel(
-    n, x_hbm, b_hbm, c_hbm, gate_hbm, resid_hbm, w_hbm,
+    n, greet, begin, x_hbm, b_hbm, c_hbm, gate_hbm, resid_hbm, w_hbm,
     step_ref, extra_ref, docrow_ref, rate_ref, direct_ref, taps_ref, btaps_ref, ctaps_ref,
     gain_ref, gain2_ref,
     mixed_ref, ffn_ref,
@@ -84,6 +84,8 @@
             pl.semaphore_signal(barrier, inc=1, device_id=(sp - off, tp), device_id_type=MESH_ID)
 
         count = count + (sp + off < n).astype(jnp.int32) + (sp >= off).astype(jnp.int32)
+    if greet is not None:
+        count = count + greet(barrier)
     pl.semaphore_wait(barrier, count)
 
     def remote(sent, received, src, dst, device):
@@ -143,6 +145,8 @@
     for load in loads[:3]:
         load.wait()
     start(edges, 1)
+    if begin is not None:
+        begin()
 
     head_row = lax.broadcasted_iota(jnp.int32, (heads, heads), 0)
     head_col = lax.broadcasted_iota(jnp.int32, (heads, heads), 1)
@@ -355,11 +359,18 @@
     ffn_ref[...] = (mixed_ref[...].astype(jnp.float32) * factor * gain2_ref[...]).astype(jnp.bfloat16)
 
 
-def mixer(n, x, b, c, gate, step, extra, rate, direct, taps, btaps, ctaps, docs, gain, resid,
-          weight, gain2):
+def mixer_operands(x, b, c, gate, step, extra, rate, direct, taps, btaps, ctaps, docs, gain, resid,
+                   weight, gain2):
+    return (x, b, c, gate, resid, weight), (
+        step.T, extra.T, docs[None, :], rate[None, :], direct[None, :], taps, btaps, ctaps,
+        gain[None, :], gain2[None, :],
+    )
+
+
+def mixer_scratch(n, x, b, c, gate, resid, weight):
     length, channels = x.shape
     state = b.shape[1]
-    half, model = resid.shape
+    half = resid.shape[0]
     hosts = HOSTS
     block = channels // hosts
     assert state == D_STATE and n % hosts == 0 and block % 128 == 0
@@ -368,45 +379,53 @@
     edge = 16
     vm = pltpu.VMEM
     sems = 4 + 3 * hosts + 4
+    return [
+        vm(x.shape, bf), vm(b.shape, bf), vm(c.shape, bf), vm(gate.shape, bf),
+        vm(resid.shape, bf), vm(weight.shape, bf), vm((length, 128), f32),
+        vm((edge + length, channels + 2 * state), f32), vm((edge + length, 128), f32),
+        vm((edge, channels), bf), vm((edge, state), bf), vm((edge, state), bf),
+        vm((edge, 128), f32),
+        vm((length, channels), bf), vm((length, state), bf), vm((length, state), bf),
+        vm((length, channels), f32), vm((length, channels), f32),
+        vm((state, channels), bf), vm((8, channels), f32),
+        vm((hosts, state, block), bf), vm((hosts, 8, block), f32),
+        vm((state, block), bf), vm((8, block), f32),
+        vm((2, state, block), bf), vm((8, block), f32),
+        vm((hosts, state, block), bf), vm((state, channels), bf),
+        vm((length, channels), bf), vm((half, channels), bf),
+        pltpu.SemaphoreType.DMA((6,)), pltpu.SemaphoreType.DMA((sems,)),
+        pltpu.SemaphoreType.DMA((sems,)),
+    ]
+
+
+def mixer(n, operands):
+    large, small = mixer_operands(*operands)
     return pl.pallas_call(
-        functools.partial(mixer_kernel, n),
-        out_shape=[jax.ShapeDtypeStruct((half, model), bf)] * 2,
-        in_specs=[pl.BlockSpec(memory_space=pl.ANY)] * 6
-        + [pl.BlockSpec(memory_space=pltpu.VMEM)] * 10,
+        functools.partial(mixer_kernel, n, None, None),
+        out_shape=[jax.ShapeDtypeStruct(large[4].shape, jnp.bfloat16)] * 2,
+        in_specs=[pl.BlockSpec(memory_space=pl.ANY)] * len(large)
+        + [pl.BlockSpec(memory_space=pltpu.VMEM)] * len(small),
         out_specs=[pl.BlockSpec(memory_space=pltpu.VMEM)] * 2,
-        scratch_shapes=[
-            vm(x.shape, bf), vm(b.shape, bf), vm(c.shape, bf), vm(gate.shape, bf),
-            vm(resid.shape, bf), vm(weight.shape, bf), vm((length, 128), f32),
-            vm((edge + length, channels + 2 * state), f32), vm((edge + length, 128), f32),
-            vm((edge, channels), bf), vm((edge, state), bf), vm((edge, state), bf),
-            vm((edge, 128), f32),
-            vm((length, channels), bf), vm((length, state), bf), vm((length, state), bf),
-            vm((length, channels), f32), vm((length, channels), f32),
-            vm((state, channels), bf), vm((8, channels), f32),
-            vm((hosts, state, block), bf), vm((hosts, 8, block), f32),
-            vm((state, block), bf), vm((8, block), f32),
-            vm((2, state, block), bf), vm((8, block), f32),
-            vm((hosts, state, block), bf), vm((state, channels), bf),
-            vm((length, channels), bf), vm((half, channels), bf),
-            pltpu.SemaphoreType.DMA((6,)), pltpu.SemaphoreType.DMA((sems,)),
-            pltpu.SemaphoreType.DMA((sems,)),
-        ],
+        scratch_shapes=mixer_scratch(n, *large),
         compiler_params=pltpu.CompilerParams(
             collective_id=0, has_side_effects=True, vmem_limit_bytes=58 * 1024 * 1024
         ),
-    )(x, b, c, gate, resid, weight, step.T, extra.T, docs[None, :], rate[None, :], direct[None, :],
-      taps, btaps, ctaps, gain[None, :], gain2[None, :])
-
-
-def plane_kernel(
-    planes, tps, ffn_ref, ids_ref, group_ref, weight_ref, mixed_ref, wg_hbm, wu_hbm, wd_hbm,
-    out_ref,
-    wg, wu, wd, meta, picks, routes, line, slots, arrived, done, back, part, mine, parts,
-    wsem, msend, mrecv, lsend, lrecv, fsend, frecv, bsend, brecv, psend, precv,
-):
+    )(*large, *small)
+
+
+def layer_kernel(planes, tps, large, small, *refs):
+    mixer_in = refs[: large + small]
+    refs = refs[large + small :]
+    ids_ref, group_ref, weight_ref, wg_hbm, wu_hbm, wd_hbm, out_ref = refs[:7]
+    (
+        mixed_ref, wg, wu, wd, meta, picks, routes, line, slots, arrived, done, back, part, mine,
+        parts,
+        wsem, msend, mrecv, lsend, lrecv, fsend, frecv, bsend, brecv, psend, precv,
+    ) = refs[7:33]
+    mixer_scratch_refs = refs[33:]
     sp = lax.axis_index("sp")
     tp = lax.axis_index("tp")
-    rows, model = ffn_ref.shape
+    rows, model = mixed_ref.shape
     per = lax.axis_size("sp") * tps // planes
     hosts = per // tps
     cap = rows // per
@@ -421,8 +440,6 @@
         pltpu.make_async_copy(wu_hbm.at[0], wu, wsem.at[1]),
         pltpu.make_async_copy(wd_hbm.at[0], wd, wsem.at[2]),
     ]
-    for load in loads:
-        load.start()
 
     def place(plane, member):
         return (plane * hosts + member // tps, member % tps)
@@ -434,13 +451,13 @@
 
         lax.fori_loop(low, high, body, 0)
 
-    barrier = pltpu.get_barrier_semaphore()
-
-    def greet(device):
-        pl.semaphore_signal(barrier, inc=1, device_id=device, device_id_type=MESH_ID)
-
-    loop(1, per, lambda d: greet(place(z, (q + d) % per)))
-    loop(1, planes, lambda d: greet(place((z + d) % planes, q)))
+    def greet(barrier):
+        def signal(device):
+            pl.semaphore_signal(barrier, inc=1, device_id=device, device_id_type=MESH_ID)
+
+        loop(1, per, lambda d: signal(place(z, (q + d) % per)))
+        loop(1, planes, lambda d: signal(place((z + d) % planes, q)))
+        return per + planes - 2
 
     def columns(c):
         return pl.ds(pl.multiple_of(c * width, width), width)
@@ -462,33 +479,39 @@
             device_id=place(z + 2 * up - 1, q), device_id_type=MESH_ID,
         )
 
-    def forward(plane, c, member):
+    peers = [
+        ((q + d) % per, place(z, (q + d) % per)) for d in range(1, per)
+    ]
+
+    def forward(plane, c, peer):
+        member, device = peer
         return pltpu.make_async_remote_copy(
             src_ref=slots.at[plane, member_rows(member), columns(c)],
             dst_ref=arrived.at[plane, member_rows(q), columns(c)],
             send_sem=fsend.at[plane], recv_sem=frecv.at[plane],
-            device_id=place(z, member), device_id_type=MESH_ID,
-        )
-
-    def backward(plane, c, member):
+            device_id=device, device_id_type=MESH_ID,
+        )
+
+    def backward(plane, c, peer):
+        member, device = peer
         return pltpu.make_async_remote_copy(
             src_ref=done.at[plane, member_rows(member), columns(c)],
             dst_ref=back.at[plane, member_rows(q), columns(c)],
             send_sem=bsend.at[plane], recv_sem=brecv.at[plane, c],
-            device_id=place(z, member), device_id_type=MESH_ID,
-        )
-
-    def home(plane, c):
+            device_id=device, device_id_type=MESH_ID,
+        )
+
+    def home(plane, c, up):
+        landing = jnp.where((up == 0) & (plane == z - 1), planes, plane)
         return pltpu.make_async_remote_copy(
-            src_ref=part.at[plane, :, columns(c)], dst_ref=parts.at[z, :, columns(c)],
-            send_sem=psend.at[plane, c], recv_sem=precv.at[z, c],
-            device_id=place(plane, q), device_id_type=MESH_ID,
-        )
-
-    def homed(plane, c):
-        return pltpu.make_async_copy(
-            parts.at[plane, :, columns(c)], parts.at[plane, :, columns(c)], precv.at[plane, c]
-        )
+            src_ref=part.at[plane, :, columns(c)], dst_ref=parts.at[landing, :, columns(c)],
+            send_sem=psend.at[plane, c], recv_sem=precv.at[landing, c],
+            device_id=place(z + 2 * up - 1, q), device_id_type=MESH_ID,
+        )
+
+    def homed(landing, c):
+        view = parts.at[landing, :, columns(c)]
+        return pltpu.make_async_copy(view, view, precv.at[landing, c])
 
     others = pl.ds(0, (per - 1) * cap)
 
@@ -500,24 +523,29 @@
         view = back.at[plane, others, columns(c)]
         return pltpu.make_async_copy(view, view, brecv.at[plane, c])
 
-    line[z] = ffn_ref[...]
-    ids = ids_ref[...]
-    group_size = experts // EXPERT_GROUPS
-    weight = jnp.zeros(ids.shape, jnp.float32)
-    for g in range(EXPERT_GROUPS):
-        inside = (ids >= g * group_size) & (ids < (g + 1) * group_size)
-        weight = weight + jnp.where(inside, group_ref[g : g + 1, :], 0.0)
-    choose = ids.shape[0]
-    info = jnp.concatenate(
-        [
-            ids.astype(jnp.float32), weight * weight_ref[...],
-            jnp.zeros((meta.shape[1] - 2 * choose, rows), jnp.float32),
-        ],
-        axis=0,
-    )
-    meta[z] = info
-    pl.semaphore_wait(barrier, per + planes - 2)
-    loop(1, planes, lambda d: tell(z, (z + d) % planes).start())
+    choose = ids_ref.shape[0]
+
+    def begin():
+        for load in loads:
+            load.start()
+        ids = ids_ref[...]
+        group_size = experts // EXPERT_GROUPS
+        weight = jnp.zeros(ids.shape, jnp.float32)
+        for g in range(EXPERT_GROUPS):
+            inside = (ids >= g * group_size) & (ids < (g + 1) * group_size)
+            weight = weight + jnp.where(inside, group_ref[g : g + 1, :], 0.0)
+        meta[z] = jnp.concatenate(
+            [
+                ids.astype(jnp.float32), weight * weight_ref[...],
+                jnp.zeros((meta.shape[1] - 2 * choose, rows), jnp.float32),
+            ],
+            axis=0,
+        )
+        loop(1, planes, lambda d: tell(z, (z + d) % planes).start())
+
+    mixer_kernel(
+        lax.axis_size("sp"), greet, begin, *mixer_in, mixed_ref, line.at[z], *mixer_scratch_refs
+    )
     for c in range(chunks):
         @pl.when(z < planes - 1)
         def _():
@@ -577,7 +605,8 @@
             picks[plane], line[plane, :, at], preferred_element_type=jnp.float32
         ).astype(jnp.bfloat16)
         arrived[plane, member_rows(q), at] = slots[plane, member_rows(q), at]
-        loop(1, per, lambda d: forward(plane, c, (q + d) % per).start())
+        for peer in peers:
+            forward(plane, c, peer).start()
 
     def stage_experts(k, plane):
         @pl.when(k == 0)
@@ -596,7 +625,8 @@
                 hidden, wd[:, at], preferred_element_type=jnp.float32
             ).astype(jnp.bfloat16)
             back[plane, member_rows(q), at] = done[plane, member_rows(q), at]
-            loop(1, per, lambda d: backward(plane, c, (q + d) % per).start())
+            for peer in peers:
+                backward(plane, c, peer).start()
 
     def stage_home(k, c, plane):
         slab(plane, c).wait()
@@ -612,7 +642,14 @@
         @pl.when(k > 0)
         def _():
             part[plane, :, at] = total.astype(jnp.bfloat16)
-            home(plane, c).start()
+
+        @pl.when((z == 0) & (k > 0))
+        def _():
+            home(plane, c, 1).start()
+
+        @pl.when((z == planes - 1) & (k > 0))
+        def _():
+            home(plane, c, 0).start()
 
     def tick(v):
         def both(k, act):
@@ -644,15 +681,47 @@
 
     loop(0, planes * chunks + lag, tick)
 
+    def pass_on(plane, c, up):
+        at = columns(c)
+        homed(plane, c).wait()
+        part[plane, :, at] = (
+            part[plane, :, at].astype(jnp.float32) + parts[plane, :, at].astype(jnp.float32)
+        ).astype(jnp.bfloat16)
+        home(plane, c, up).start()
+
+    behind = 1
+
+    def relay(v):
+        def serve(w, up):
+            reach = 1 + w // chunks
+            plane = jnp.where(up == 1, reach, planes - 1 - reach)
+            valid = jnp.where(up == 1, (plane > z) & (z > 0), (plane < z) & (z < planes - 1))
+
+            @pl.when(valid & (w >= 0) & (w < (planes - 1) * chunks))
+            def _():
+                pass_on(plane, w % chunks, up)
+
+        leading = jnp.where(2 * z < planes, 1, 0)
+        loop(0, 2, lambda i: serve(v - i * behind, jnp.where(i == 0, leading, 1 - leading)))
+
+    loop(0, (planes - 1) * chunks + behind, relay)
+
     for c in range(chunks):
         at = slice(c * width, (c + 1) * width)
-        loop(1, planes, lambda d: homed((z + d) % planes, c).wait())
         mine[:, at] = mine[:, at] + mixed_ref[:, at].astype(jnp.float32)
 
-        def add(d):
-            mine[:, at] = mine[:, at] + parts[(z + d) % planes, :, at].astype(jnp.float32)
-
-        loop(1, planes, add)
+        def add(landing):
+            homed(landing, c).wait()
+            mine[:, at] = mine[:, at] + parts[landing, :, at].astype(jnp.float32)
+
+        @pl.when(z > 0)
+        def _():
+            add(z)
+
+        @pl.when(z < planes - 1)
+        def _():
+            add(planes)
+
         out_ref[:, at] = mine[:, at].astype(jnp.bfloat16)
 
     loop(1, planes, lambda d: tell(z, (z + d) % planes).wait_send())
@@ -672,27 +741,30 @@
 
             @pl.when(plane != z)
             def _():
-                home(plane, c).wait_send()
+                home(plane, c, 1).wait_send()
 
         loop(0, chunks, each)
 
     loop(0, planes, finish)
 
 
-def exchange(ffn, ids, group_weight, chosen_weight, mixed, gate_weight, up_weight, down_weight,
-             planes):
-    rows, model = ffn.shape
+def layer(n, operands, ids, group_weight, chosen_weight, gate_weight, up_weight, down_weight,
+          planes):
+    large, small = mixer_operands(*operands)
+    rows, model = large[4].shape
     chunks = 4
     bf, f32 = jnp.bfloat16, jnp.float32
     vm = pltpu.VMEM
     dma = pltpu.SemaphoreType.DMA
     return pl.pallas_call(
-        functools.partial(plane_kernel, planes, lax.axis_size("tp")),
-        out_shape=jax.ShapeDtypeStruct(mixed.shape, bf),
-        in_specs=[pl.BlockSpec(memory_space=pltpu.VMEM)] * 5
+        functools.partial(layer_kernel, planes, lax.axis_size("tp"), len(large), len(small)),
+        out_shape=jax.ShapeDtypeStruct((rows, model), bf),
+        in_specs=[pl.BlockSpec(memory_space=pl.ANY)] * len(large)
+        + [pl.BlockSpec(memory_space=pltpu.VMEM)] * (len(small) + 3)
         + [pl.BlockSpec(memory_space=pl.ANY)] * 3,
         out_specs=pl.BlockSpec(memory_space=pltpu.VMEM),
         scratch_shapes=[
+            vm((rows, model), bf),
             vm(gate_weight.shape[1:], bf), vm(up_weight.shape[1:], bf),
             vm(down_weight.shape[1:], bf),
             vm((planes, 8, rows), f32),
@@ -700,16 +772,16 @@
             vm((planes, rows, model), bf), vm((planes, rows, model), bf),
             vm((planes, rows, model), bf), vm((planes, rows, model), bf),
             vm((planes, rows, model), bf), vm((planes, rows, model), bf),
-            vm((rows, model), f32), vm((planes, rows, model), bf),
+            vm((rows, model), f32), vm((planes + 1, rows, model), bf),
             dma((3,)), dma((planes,)), dma((planes,)),
             dma((2, planes, chunks)), dma((planes, chunks)),
             dma((planes,)), dma((planes,)), dma((planes,)), dma((planes, chunks)),
-            dma((planes, chunks)), dma((planes, chunks)),
-        ],
+            dma((planes, chunks)), dma((planes + 1, chunks)),
+        ] + mixer_scratch(n, *large),
         compiler_params=pltpu.CompilerParams(
-            collective_id=1, has_side_effects=True, vmem_limit_bytes=56 * 1024 * 1024
+            collective_id=1, has_side_effects=True, vmem_limit_bytes=62 * 1024 * 1024
         ),
-    )(ffn, ids, group_weight, chosen_weight, mixed, gate_weight, up_weight, down_weight)
+    )(*large, *small, ids, group_weight, chosen_weight, gate_weight, up_weight, down_weight)
 
 
 def local(
@@ -736,25 +808,27 @@
     expert_up_weight,
     expert_down_weight,
 ):
-    mixed_rows, ffn_in = mixer(
-        lax.axis_size("sp"), mixer_value_rows, input_map_rows, output_map_rows,
-        gate_preactivation, step_preactivation, position_extra_decay, head_decay_rate,
-        head_direct_term, value_taps, input_map_taps, output_map_taps, document_index,
-        gated_norm_gain, residual, mixer_output_weight, expert_norm_gain,
-    )
-    experts = lax.axis_size("sp") * lax.axis_size("tp")
-    row_count, width = ffn_in.shape
+    operands = (
+        mixer_value_rows, input_map_rows, output_map_rows, gate_preactivation, step_preactivation,
+        position_extra_decay, head_decay_rate, head_direct_term, value_taps, input_map_taps,
+        output_map_taps, document_index, gated_norm_gain, residual, mixer_output_weight,
+        expert_norm_gain,
+    )
+    hosts, tps = lax.axis_size("sp"), lax.axis_size("tp")
+    experts = hosts * tps
+    row_count, width = residual.shape
     choose = chosen_expert_index.shape[1]
     capacity = 2 * mixer_value_rows.shape[0] // experts
     per = row_count // capacity
     if (
         capacity % 16 == 0 and row_count % capacity == 0 and experts % per == 0
-        and per % lax.axis_size("tp") == 0 and experts % EXPERT_GROUPS == 0 and choose <= 4
+        and per % tps == 0 and experts % EXPERT_GROUPS == 0 and choose <= 4 and experts >= 2 * per
     ):
-        return exchange(
-            ffn_in, chosen_expert_index.T, expert_group_weight.T, chosen_expert_weight.T,
-            mixed_rows, expert_gate_weight, expert_up_weight, expert_down_weight, experts // per,
-        )
+        return layer(
+            hosts, operands, chosen_expert_index.T, expert_group_weight.T, chosen_expert_weight.T,
+            expert_gate_weight, expert_up_weight, expert_down_weight, experts // per,
+        )
+    mixed_rows, ffn_in = mixer(hosts, operands)
     ids = jnp.arange(experts, dtype=jnp.int32)
     chosen = (chosen_expert_index[:, :, None] == ids).astype(jnp.bfloat16)
     named = jnp.sum(chosen, axis=1)

time: 124 us -> 117 us (0.944)
  Pallas kernels: 122 us -> 115 us
    pallas_call x2 -> x1, Pallas kernels: 122 us -> 115 us  [layer(): pl.pallas_call(functools.partial(layer_kernel, planes, lax.axis_size('tp'...]
where the time goes in v3:
time: 117 us
  Pallas kernels  115 us (98%)
  local copies, waits for them, and re-layouts  1.88 us (2%)
    pallas_call x1, Pallas kernels, layer(): pl.pallas_call(functools.partial(layer_kernel, planes, lax.axis_size('tp'...  115 us

profile of v3, /device:TPU:0, one launch (start us, length us, event | category | flops | bytes accessed | tf_op | source)
XLA Modules:
  0.0 116.9 jit_solution(461955845961642568)
XLA Ops:
  0.0 115.0 %shard_map.208 = bf16[128,2048]{1,0:T(8,128)(2,1)} custom-call(bf16[256,1024]{1,0:T(8,128)(2,1)} %refs_0_.1, bf16[256,128]{1,0:T(8,128)(2,1)} %refs_1_.1, bf16[256,128]{1,0:T(8,128)(2,1)} %refs_2_.1, bf16[256,1024]{1,0:T(8,128)(2,1)} %refs_3_.1, bf16[128,2048]{1,0:T(8,128)(2,1)} %refs_4_.1, bf16[2048,2048]{1,0:T(8,128)(2,1)} %refs_5_.1, f32[16,256]{1,0:T(8,128)} %bitcast.10, ...), custom_call_target="tpu_custom_call" | custom-call | tf_op jit(solution)/shard_map/pallas_call | solution.py:759
  115.0 1.9 %copy.24 = bf16[128,2048]{1,0:T(8,128)(2,1)} copy(bf16[128,2048]{1,0:T(8,128)(2,1)} %shard_map.208) | data formatting | bytes 1048576

commit v4 on v3

--- a/solution.py
+++ b/solution.py
@@ -215,17 +215,26 @@
         at = spread_lane + j * lanes - spread_row
         return jnp.where((at >= 0) & (at < width), 1.0, 0.0)
 
+    lane = lax.broadcasted_iota(jnp.int32, (length, lanes), 1)
+    step_columns = jnp.transpose(
+        jnp.concatenate([step, jnp.zeros((lanes - heads, length), jnp.float32)], axis=0)
+    )
+
+    def spread(columns, j):
+        result = None
+        for k in range(per_chunk):
+            h = j * per_chunk + k
+            part = jnp.broadcast_to(columns[:, h : h + 1], (length, lanes))
+            result = part if result is None else jnp.where(lane < k * width, result, part)
+        return result
+
     for j in range(chunks):
         at = slice(j * lanes, (j + 1) * lanes)
         value = conv(j * lanes, taps_ref, j * lanes)
         vconv[:, at] = value
-        wide = widen(j)
-        cum_wide = exact_dot(cum, wide)
+        cum_wide = spread(cum, j)
         cumx[:, at] = cum_wide
-        step_wide = lax.dot_general(
-            step, wide, (((0,), (0,)), ((), ())),
-            preferred_element_type=jnp.float32, precision=lax.Precision.HIGHEST,
-        )
+        step_wide = spread(step_columns, j)
         stepped = (step_wide * value.astype(jnp.float32)).astype(jnp.bfloat16)
         ylocal[:, at] = stepped.astype(jnp.float32)
         ending = cum_wide[length - 1 : length, :]
@@ -249,7 +258,6 @@
     scores = lax.dot_general(
         cconv[...], bconv[...], (((1,), (1,)), ((), ())), preferred_element_type=jnp.float32
     )
-    lane = lax.broadcasted_iota(jnp.int32, (length, lanes), 1)
 
     def inside(j):
         at = slice(j * lanes, (j + 1) * lanes)
@@ -577,7 +585,7 @@
         picks[plane] = hot.astype(jnp.bfloat16)
         routes[plane] = jnp.transpose(hot * value).astype(jnp.bfloat16)
 
-    lag = chunks + 2
+    lag = chunks + 1
 
     def stage_rows(k, c, up, plane):
         @pl.when(k > 0)

time: 117 us -> 115 us (0.983)
  Pallas kernels: 115 us -> 113 us
    pallas_call x1, Pallas kernels: 115 us -> 113 us  [layer(): pl.pallas_call(functools.partial(layer_kernel, planes, lax.axis_size('tp'...]
where the time goes in v4:
time: 115 us
  Pallas kernels  113 us (98%)
  local copies, waits for them, and re-layouts  1.88 us (2%)
    pallas_call x1, Pallas kernels, layer(): pl.pallas_call(functools.partial(layer_kernel, planes, lax.axis_size('tp'...  113 us

profile of v4, /device:TPU:0, one launch (start us, length us, event | category | flops | bytes accessed | tf_op | source)
XLA Modules:
  0.0 115.3 jit_solution(3753200344070900928)
XLA Ops:
  0.0 113.4 %shard_map.208 = bf16[128,2048]{1,0:T(8,128)(2,1)} custom-call(bf16[256,1024]{1,0:T(8,128)(2,1)} %refs_0_.1, bf16[256,128]{1,0:T(8,128)(2,1)} %refs_1_.1, bf16[256,128]{1,0:T(8,128)(2,1)} %refs_2_.1, bf16[256,1024]{1,0:T(8,128)(2,1)} %refs_3_.1, bf16[128,2048]{1,0:T(8,128)(2,1)} %refs_4_.1, bf16[2048,2048]{1,0:T(8,128)(2,1)} %refs_5_.1, f32[16,256]{1,0:T(8,128)} %bitcast.10, ...), custom_call_target="tpu_custom_call" | custom-call | tf_op jit(solution)/shard_map/pallas_call | solution.py:767
  113.4 1.9 %copy.24 = bf16[128,2048]{1,0:T(8,128)(2,1)} copy(bf16[128,2048]{1,0:T(8,128)(2,1)} %shard_map.208) | data formatting | bytes 1048576
